TPU v7x, 32 devices: a whole 2x2x4 slice. The times are simulated.
32 devices in a mesh: grp: 2 (over y), fs: 4 (over z), tp: 4 (over x, core).
Axes of the slice: x: 2, y: 2, z: 4, core: 2. Of those that a mesh axis runs over, the one named last changes fastest.
Arguments:
- tokens: bfloat16 [4096, 2048], P(('grp', 'fs', 'tp')), parts along dimension 0, may hold values from -6 to 6
- mix_weight_in: bfloat16 [2048, 1024], P('fs', 'tp'), may hold values from -0.125 to 0.125
- pool_scale: float32 [1024], P('tp'), may hold values from 0.1 to 1.9
- mix_weight_out: bfloat16 [1024, 2048], P('tp', 'fs'), may hold values from -0.1875 to 0.1875
- up_weight: bfloat16 [2048, 8192], P('fs', 'tp'), may hold values from -0.125 to 0.125
- down_weight: bfloat16 [8192, 2048], P('tp', 'fs'), may hold values from -0.0625 to 0.0625
- gains: float32 [4, 2048], replicated, may hold values from 0.1 to 1.9
Outputs:
- result: bfloat16 [4096, 2048], P(('grp', 'fs', 'tp')), parts along dimension 0
There are 2 independent parts, one for each index of `grp`. A program takes and returns all parts, laid end to end along the dimension named above; an argument that names none is the same for every part. Nothing has to cross between parts.
All inputs are finite; a program needn't handle non-finite values.
Results may differ from a plain program's by a relative error of at most 0.02.
Values may be sent and summed in bfloat16 or wider, within the bound.
No kernel may reach another device: no remote copies, remote signals or barrier semaphores. Data moves between devices by JAX's collectives and lax.ppermute only.
A program may use at most 64 MiB of HBM per device.

v0:
```python
import jax
import jax.numpy as jnp
from jax import lax
from jax.sharding import PartitionSpec as P

PW = 1024
GROUPS = 4


norm_eps = 1e-06
pool_spans = (2, 4, 8, 16)


def normalize(values, gain):
    upcast = values.astype(jnp.float32)
    return upcast * lax.rsqrt(jnp.mean(upcast * upcast, axis=-1, keepdims=True) + norm_eps) * gain


def pooling(mixed_in, first_channel):
    length = mixed_in.shape[0]
    upcast = mixed_in.astype(jnp.float32)
    running = jnp.cumsum(upcast, axis=0)
    position = jnp.arange(1, length + 1, dtype=jnp.float32)[:, None]
    channel = first_channel + jnp.arange(mixed_in.shape[1], dtype=jnp.int32)
    group_of = (channel // (PW // GROUPS))[None, :]
    average = jnp.zeros_like(upcast)
    for index, span in enumerate(pool_spans):
        lagged = jnp.pad(running, ((span, 0), (0, 0)))[:length]
        window_mean = (running - lagged) / jnp.minimum(position, float(span))
        average = jnp.where(group_of == index, window_mean, average)
    return average - upcast


def local(tokens, mix_weight_in, pool_scale, mix_weight_out, up_weight, down_weight, gains):
    normed = normalize(tokens, gains[0]).astype(jnp.bfloat16)
    gathered = lax.all_gather(normed, "tp", axis=0, tiled=True)
    mixed_acc = jnp.dot(
        gathered,
        lax.all_gather(mix_weight_in, "fs", axis=0, tiled=True),
        preferred_element_type=jnp.float32,
    )
    weight_out = lax.all_gather(mix_weight_out, "fs", axis=1, tiled=True)
    mixed_in = mixed_acc.astype(jnp.bfloat16)
    first_channel = lax.axis_index("tp") * mix_weight_in.shape[1]
    scaled = (pooling(mixed_in, first_channel) * pool_scale).astype(jnp.bfloat16)
    picked = scaled
    mixer_out = lax.psum_scatter(
        jnp.dot(picked, weight_out, preferred_element_type=jnp.float32).astype(jnp.bfloat16),
        "tp",
        scatter_dimension=0,
        tiled=True,
    )
    middle = (tokens.astype(jnp.float32) + normalize(mixer_out, gains[1])).astype(jnp.bfloat16)
    normed_two = normalize(middle, gains[2]).astype(jnp.bfloat16)
    gathered_two = lax.all_gather(normed_two, "tp", axis=0, tiled=True)
    whole_up = lax.all_gather(up_weight, "fs", axis=0, tiled=True)
    hidden_pre = jnp.dot(gathered_two, whole_up, preferred_element_type=jnp.float32)
    hidden_pre = jax.nn.relu(hidden_pre)
    squared = (hidden_pre * hidden_pre).astype(jnp.bfloat16)
    whole_down = lax.all_gather(down_weight, "fs", axis=1, tiled=True)
    picked = squared
    channel_out = lax.psum_scatter(
        jnp.dot(picked, whole_down, preferred_element_type=jnp.float32).astype(jnp.bfloat16),
        "tp",
        scatter_dimension=0,
        tiled=True,
    )
    return (middle.astype(jnp.float32) + normalize(channel_out, gains[3])).astype(jnp.bfloat16)


def solution(mesh):
    return jax.shard_map(
        local,
        mesh=mesh,
        in_specs=(
            P(("grp", "fs", "tp"), None),
            P("fs", "tp"),
            P("tp"),
            P("tp", "fs"),
            P("fs", "tp"),
            P("tp", "fs"),
            P(),
        ),
        out_specs=P(("grp", "fs", "tp"), None),
        check_vma=False,
    )
```

profile of v0, /device:TPU:0, one launch (start us, length us, event | category | flops | bytes accessed | tf_op | source)
XLA Modules:
  0.0 510.2 jit_solution(9647239780460896980)
XLA Ops:
  6.5 0.0 all-gather.9.cloned.1.call-start
  6.5 0.7 all-gather.9.cloned.1.call-update
  7.3 0.0 all-gather.7.cloned.1.call-start
  7.3 1.2 fusion.5
  8.5 0.9 fusion.48
  9.5 2.0 fusion.7
  11.5 0.0 all-gather.7.cloned.1.call-update
  11.5 0.0 all-gather.11.cloned.1.call-start
  11.6 0.7 all-gather.11.cloned.1.call-update
  12.3 0.0 reduce-scatter.3.cloned.1.call-start
  12.4 27.2 %all-gather.9.cloned.1.call-done = bf16[2048,256]{1,0:T(8,128)(2,1)} async-done(((bf16[512,256]{1,0:T(8,128)(2,1)}), bf16[2048,256]{1,0:T(8,128)(2,1)}) %all-gather.9.cloned.1.call-update) | async-done | bytes 1048592 | tf_op jit(solution)/shard_map/all_gather | solution.py:39
  39.6 23.5 %all-gather.7.cloned.1.call-done = bf16[512,2048]{1,0:T(8,128)(2,1)} async-done(((bf16[128,2048]{1,0:T(8,128)(2,1)}), bf16[512,2048]{1,0:T(8,128)(2,1)}) %all-gather.7.cloned.1.call-update) | async-done | bytes 2097168 | tf_op jit(solution)/shard_map/all_gather | solution.py:36
  63.2 2.6 fusion
  65.7 0.0 copy-start.1
  65.8 0.3 fusion.27
  66.2 0.1 copy.9
  66.3 26.5 %all-gather.11.cloned.1.call-done = bf16[256,2048]{1,0:T(8,128)(2,1)} async-done(((bf16[256,512]{1,0:T(8,128)(2,1)}), bf16[256,2048]{1,0:T(8,128)(2,1)}) %all-gather.11.cloned.1.call-update) | async-done | bytes 1048592 | tf_op jit(solution)/shard_map/all_gather | solution.py:42
  92.8 0.0 copy-done.1
  92.8 3.6 convolution_convert_fusion
  96.3 0.0 copy-start
  96.3 0.0 reduce-scatter.3.cloned.1.call-update
  96.3 0.0 all-gather.13.cloned.1.call-start
  96.4 30.7 %reduce-scatter.3.cloned.1.call-done = bf16[128,2048]{1,0:T(8,128)(2,1)} async-done(((bf16[512,2048]{1,0:T(8,128)(2,1)}), bf16[128,2048]{1,0:T(8,128)(2,1)}) %reduce-scatter.3.cloned.1.call-update) | async-done | bytes 524304 | tf_op jit(solution)/shard_map/reduce_scatter | solution.py:47
  127.1 1.2 fusion.1
  128.3 0.0 copy-done
  128.3 1.5 fusion.9
  129.8 1.0 fusion.11
  130.8 0.0 all-gather.13.cloned.1.call-update
  130.8 0.0 all-gather.15.cloned.1.call-start
  130.8 0.5 all-gather.15.cloned.1.call-update
  131.4 0.0 all-gather.17.cloned.1.call-start
  131.4 0.7 all-gather.17.cloned.1.call-update
  132.1 0.0 reduce-scatter.5.cloned.1.call-start
  132.2 21.3 %all-gather.13.cloned.1.call-done = bf16[512,2048]{1,0:T(8,128)(2,1)} async-done(((bf16[128,2048]{1,0:T(8,128)(2,1)}), bf16[512,2048]{1,0:T(8,128)(2,1)}) %all-gather.13.cloned.1.call-update) | async-done | bytes 2097168 | tf_op jit(solution)/shard_map/all_gather | solution.py:55
  153.5 151.1 %all-gather.15.cloned.1.call-done = bf16[2048,2048]{1,0:T(8,128)(2,1)} async-done(((bf16[512,2048]{1,0:T(8,128)(2,1)}), bf16[2048,2048]{1,0:T(8,128)(2,1)}) %all-gather.15.cloned.1.call-update) | async-done | bytes 8388624 | tf_op jit(solution)/shard_map/all_gather | solution.py:56
  304.6 149.4 %all-gather.17.cloned.1.call-done = bf16[2048,2048]{1,0:T(8,128)(2,1)} async-done(((bf16[2048,512]{1,0:T(8,128)(2,1)}), bf16[2048,2048]{1,0:T(8,128)(2,1)}) %all-gather.17.cloned.1.call-update) | async-done | bytes 8388624 | tf_op jit(solution)/shard_map/all_gather | solution.py:60
  454.0 16.5 %convolution_convert_fusion.1 = bf16[512,2048]{1,0:T(8,128)(2,1)} fusion(bf16[2048,2048]{1,0:T(8,128)(2,1)} %all-gather.17.cloned.1.call-done, bf16[512,2048]{1,0:T(8,128)(2,1)} %all-gather.13.cloned.1.call-done, bf16[2048,2048]{1,0:T(8,128)(2,1)} %all-gather.15.cloned.1.call-done), kind=kOutput, calls=%fused_computation.2 | convolution fusion | flops 8594128896 | bytes 20971520 | tf_op jit(solution)/shard_map/dot_general | solution.py:63
  470.5 0.0 reduce-scatter.5.cloned.1.call-update
  470.5 29.5 %reduce-scatter.5.cloned.1.call-done = bf16[128,2048]{1,0:T(8,128)(2,1)} async-done(((bf16[512,2048]{1,0:T(8,128)(2,1)}), bf16[128,2048]{1,0:T(8,128)(2,1)}) %reduce-scatter.5.cloned.1.call-update) | async-done | bytes 524304 | tf_op jit(solution)/shard_map/reduce_scatter | solution.py:62
  500.0 1.2 fusion.3
  501.3 2.1 fusion.12
  (13 shorter events, 0.2 us)
Async XLA Ops:
  6.5 33.1 %all-gather.9.cloned.1.call-start = ((), (), s32[]{:S(2)}) async-start(), calls=%async_computation.3 | async-start | bytes 1310720 | tf_op jit(solution)/shard_map/all_gather | solution.py:39
  7.3 55.9 %all-gather.7.cloned.1.call-start = ((), (), s32[]{:S(2)}) async-start(), calls=%async_computation.2 | async-start | bytes 2621440 | tf_op jit(solution)/shard_map/all_gather | solution.py:36
  11.5 81.2 %all-gather.11.cloned.1.call-start = ((), (), s32[]{:S(2)}) async-start(), calls=%async_computation.4 | async-start | bytes 1310720 | tf_op jit(solution)/shard_map/all_gather | solution.py:42
  12.3 114.8 %reduce-scatter.3.cloned.1.call-start = ((), (), s32[]{:S(2)}) async-start(), calls=%async_computation.5 | async-start | bytes 2621440 | tf_op jit(solution)/shard_map/reduce_scatter | solution.py:47
  65.7 27.0 %copy-start.1 = (f32[256]{0:T(256)S(1)}, f32[256]{0:T(256)}, u32[]{:S(2)}) copy-start(f32[256]{0:T(256)} %param.9) | copy-start | bytes 3076
  96.3 32.0 %copy-start = (bf16[128,2048]{1,0:T(8,128)(2,1)S(1)}, bf16[128,2048]{1,0:T(8,128)(2,1)}, u32[]{:S(2)}) copy-start(bf16[128,2048]{1,0:T(8,128)(2,1)} %param.7) | copy-start | bytes 1572868
  96.3 57.1 %all-gather.13.cloned.1.call-start = ((), (), s32[]{:S(2)}) async-start(), calls=%async_computation.6 | async-start | bytes 2621440 | tf_op jit(solution)/shard_map/all_gather | solution.py:55
  130.8 173.8 %all-gather.15.cloned.1.call-start = ((), (), s32[]{:S(2)}) async-start(), calls=%async_computation.7 | async-start | bytes 10485760 | tf_op jit(solution)/shard_map/all_gather | solution.py:56
  131.4 322.6 %all-gather.17.cloned.1.call-start = ((), (), s32[]{:S(2)}) async-start(), calls=%async_computation.8 | async-start | bytes 10485760 | tf_op jit(solution)/shard_map/all_gather | solution.py:60
  132.1 367.9 %reduce-scatter.5.cloned.1.call-start = ((), (), s32[]{:S(2)}) async-start(), calls=%async_computation.9 | async-start | bytes 2621440 | tf_op jit(solution)/shard_map/reduce_scatter | solution.py:62
Sparse Core Ops, SparseCore 0:
  8.9 30.6 all-gather.8
  41.2 21.9 all-gather.6
  64.7 27.9 all-gather.10
  96.5 30.5 reduce-scatter.2
  130.9 22.5 all-gather.12
  154.9 149.6 all-gather.14
  306.1 147.7 all-gather.16
  470.6 29.3 reduce-scatter.4
where the time goes:
time: 511 us; the launch traced here: 510 us
  waiting for transfers between devices  462 us (90%)
  matrix products  22.6 us (4%)
  between operations  13.6 us (3%)
  other arithmetic  10.8 us (2%)
    all_gather x1, waiting for transfers between devices, local(): whole_up = lax.all_gather(up_weight, 'fs', axis=0, tiled=True)  151 us
    all_gather x1, waiting for transfers between devices, local(): whole_down = lax.all_gather(down_weight, 'fs', axis=1, tiled=True)  149 us
    reduce_scatter x1, waiting for transfers between devices, local(): lax.psum_scatter(jnp.dot(picked, weight_out, preferred_element_type=jnp.f...  30.7 us
    reduce_scatter x1, waiting for transfers between devices, local(): lax.psum_scatter(jnp.dot(picked, whole_down, preferred_element_type=jnp.f...  29.5 us
    all_gather x1, waiting for transfers between devices, local(): lax.all_gather(mix_weight_in, 'fs', axis=0, tiled=True)  27.2 us
    all_gather x1, waiting for transfers between devices, local(): weight_out = lax.all_gather(mix_weight_out, 'fs', axis=1, tiled=True)  26.5 us
    all_gather x1, waiting for transfers between devices, local(): gathered = lax.all_gather(normed, 'tp', axis=0, tiled=True)  23.5 us
    all_gather x1, waiting for transfers between devices, local(): gathered_two = lax.all_gather(normed_two, 'tp', axis=0, tiled=True)  21.3 us
  transfers between devices with their start and end apart: 8, of which 8 were waited for; matrix products, arithmetic and copies ran while one was open for 1% of the time, Pallas kernels for 0%

commit v1 on v0

--- a/solution.py
+++ b/solution.py
@@ -6,9 +6,11 @@
 PW = 1024
 GROUPS = 4
 
-
 norm_eps = 1e-06
 pool_spans = (2, 4, 8, 16)
+
+
+f32, bf16 = jnp.float32, jnp.bfloat16
 
 
 def normalize(values, gain):
@@ -31,7 +33,7 @@
     return average - upcast
 
 
-def local(tokens, mix_weight_in, pool_scale, mix_weight_out, up_weight, down_weight, gains):
+def whole_axis(tokens, mix_weight_in, pool_scale, mix_weight_out, up_weight, down_weight, gains):
     normed = normalize(tokens, gains[0]).astype(jnp.bfloat16)
     gathered = lax.all_gather(normed, "tp", axis=0, tiled=True)
     mixed_acc = jnp.dot(
@@ -68,9 +70,141 @@
     return (middle.astype(jnp.float32) + normalize(channel_out, gains[3])).astype(jnp.bfloat16)
 
 
+def rsqrt_mean(blocks, width):
+    total = sum(jnp.sum(b.astype(f32) * b.astype(f32), axis=-1, keepdims=True) for b in blocks)
+    return lax.rsqrt(total / width + norm_eps)
+
+
+def dot(a, b):
+    return jnp.dot(a, b, preferred_element_type=f32)
+
+
+def make_local(n_grp, n_fs, n_tp):
+    def swap(value, axis, n, bit):
+        return lax.ppermute(value, axis, [(i, i ^ bit) for i in range(n)])
+
+    def local(tokens, mix_in, pool_scale, mix_out, up, down, gains):
+        g, z, t = lax.axis_index("grp"), lax.axis_index("fs"), lax.axis_index("tp")
+        rows, width = tokens.shape
+        col = width // n_fs
+        channels = mix_in.shape[1]
+        part = channels // n_grp
+        ff = up.shape[1] // n_grp
+
+        def slots(value):
+            blocks = [value[..., k * col:(k + 1) * col] for k in range(n_fs)]
+            for bit in (2, 1):
+                blocks = [jnp.where((z & bit) != 0, blocks[k ^ bit], blocks[k]) for k in range(n_fs)]
+            return blocks
+
+        def gather_fs(value):
+            two = swap(value, "fs", n_fs, 2)
+            one = swap(value, "fs", n_fs, 1)
+            three = swap(two, "fs", n_fs, 1)
+            return [value, one, two, three]
+
+        mi = gather_fs(lax.dynamic_slice_in_dim(mix_in, g * part, part, axis=1))
+        mo = gather_fs(lax.dynamic_slice_in_dim(mix_out, g * part, part, axis=0))
+        up = gather_fs(lax.dynamic_slice_in_dim(up, g * ff, ff, axis=1))
+        down = lax.dynamic_slice_in_dim(down, g * ff, ff, axis=0)
+        down_a = gather_fs(down[:, :col // 2])
+        down_b = gather_fs(down[:, col // 2:])
+
+        w_in = jnp.concatenate(mi, axis=0)
+        w_in = jnp.concatenate([w_in, swap(w_in, "grp", n_grp, 1)], axis=1)
+        w_out = jnp.concatenate(mo, axis=1)
+        w_out = jnp.concatenate([w_out, swap(w_out, "grp", n_grp, 1)], axis=0)
+
+        gain = [slots(gains[k:k + 1]) for k in range(4)]
+        x = slots(tokens)
+        r = rsqrt_mean([tokens], width)
+        normed = jnp.concatenate([(x[j].astype(f32) * r * gain[0][j]).astype(bf16) for j in range(n_fs)], axis=1)
+        gathered = jnp.concatenate([normed, swap(normed, "tp", n_tp, 2)], axis=0)
+        gathered = jnp.concatenate([gathered, swap(gathered, "tp", n_tp, 1)], axis=0)
+        order = (0, 2, 1, 3)
+
+        scale = [lax.dynamic_slice_in_dim(pool_scale, (g ^ k) * part, part) for k in range(n_grp)]
+        scale = jnp.concatenate(scale)[None, :]
+        index = jnp.arange(rows, dtype=jnp.int32)
+        position = jnp.concatenate([(t ^ k) * rows + index for k in order])
+        group = PW // GROUPS
+        mine = (t * channels) // group
+        span = jnp.int32(pool_spans[0])
+        for k in range(1, GROUPS):
+            span = jnp.where(mine == k, pool_spans[k], span)
+        lag = position[:, None] - position[None, :]
+        ones = ((lag >= 0) & (lag < span)).astype(bf16)
+        count = jnp.minimum(position + 1, span).astype(f32)[:, None]
+
+        mixed = dot(gathered, w_in).astype(bf16)
+        average = dot(ones, mixed) / count
+        scaled = ((average - mixed.astype(f32)) * scale).astype(bf16)
+        half = 2 * rows
+        sent = swap(dot(scaled[half:], w_out).astype(bf16), "tp", n_tp, 1)
+        partial = (dot(scaled[:half], w_out) + sent.astype(f32)).astype(bf16)
+        sent = swap(partial[rows:], "tp", n_tp, 2)
+        partial = (partial[:rows].astype(f32) + sent.astype(f32)).astype(bf16)
+
+        mixer_out = [partial[:, k * col:(k + 1) * col] for k in range(n_fs)]
+        r = rsqrt_mean(mixer_out, width)
+        middle = [(x[j].astype(f32) + mixer_out[j].astype(f32) * r * gain[1][j]).astype(bf16) for j in range(n_fs)]
+        r = rsqrt_mean(middle, width)
+        normed_two = [(middle[j].astype(f32) * r * gain[2][j]).astype(bf16) for j in range(n_fs)]
+
+        left = jnp.concatenate(normed_two[:2], axis=1)
+        right = jnp.concatenate(normed_two[2:], axis=1)
+        left = jnp.concatenate([left, swap(left, "tp", n_tp, 2)], axis=0)
+        left_far = swap(left, "grp", n_grp, 1)
+        right_grp = swap(right, "grp", n_grp, 1)
+        right_far = swap(jnp.concatenate([right, right_grp], axis=0), "tp", n_tp, 2)
+        chips = jnp.concatenate(
+            [
+                jnp.concatenate([left, left_far], axis=0),
+                jnp.concatenate([right, right_far[:rows], right_grp, right_far[rows:]], axis=0),
+            ],
+            axis=1,
+        )
+        everything = jnp.concatenate([chips, swap(chips, "tp", n_tp, 1)], axis=0)
+
+        hidden = sum(dot(everything[:, j * col:(j + 1) * col], up[j]) for j in range(n_fs))
+        hidden = jnp.maximum(hidden, 0.0)
+        squared = (hidden * hidden).astype(bf16)
+
+        def add_up(weights):
+            half = 4 * rows
+            sent = jnp.concatenate([dot(squared[half:], w).astype(bf16) for w in weights], axis=1)
+            got = swap(sent, "tp", n_tp, 1)
+            spans, at = [], 0
+            for w in weights:
+                spans.append((at, at + w.shape[1]))
+                at += w.shape[1]
+            total = [(dot(squared[:half], w) + got[:, a:b].astype(f32)).astype(bf16) for w, (a, b) in zip(weights, spans)]
+            got = swap(jnp.concatenate([v[half // 2:] for v in total], axis=1), "grp", n_grp, 1)
+            total = [(v[:half // 2].astype(f32) + got[:, a:b].astype(f32)).astype(bf16) for v, (a, b) in zip(total, spans)]
+            got = swap(jnp.concatenate([v[rows:] for v in total], axis=1), "tp", n_tp, 2)
+            return [(v[:rows].astype(f32) + got[:, a:b].astype(f32)).astype(bf16) for v, (a, b) in zip(total, spans)]
+
+        first = add_up([down, down_a[1], down_a[2]])
+        second = add_up([down_b[1], down_b[2], down_a[3]])
+        third = add_up([down_b[3]])
+        channel_out = [
+            first[0],
+            jnp.concatenate([first[1], second[0]], axis=1),
+            jnp.concatenate([first[2], second[1]], axis=1),
+            jnp.concatenate([second[2], third[0]], axis=1),
+        ]
+        r = rsqrt_mean(channel_out, width)
+        result = [(middle[j].astype(f32) + channel_out[j].astype(f32) * r * gain[3][j]).astype(bf16) for j in range(n_fs)]
+        return jnp.concatenate(slots(jnp.concatenate(result, axis=1)), axis=1)
+
+    return local
+
+
 def solution(mesh):
+    n_grp, n_fs, n_tp = (mesh.shape[name] for name in ("grp", "fs", "tp"))
+    small = (n_grp, n_fs, n_tp) == (2, 4, 4)
     return jax.shard_map(
-        local,
+        make_local(n_grp, n_fs, n_tp) if small else whole_axis,
         mesh=mesh,
         in_specs=(
             P(("grp", "fs", "tp"), None),

time: 511 us -> 293 us (0.57)
  waiting for transfers between devices: 462 us -> 194 us
  starting transfers between devices: 0.28 us -> 41 us
  other arithmetic: 10.8 us -> 32.5 us
  between operations: 13.6 us -> 0.73 us
    all_gather x6 -> x0, waiting for transfers between devices: 399 us -> none  [the longest x1 151 us: local(): whole_up = lax.all_gather(up_weight, 'fs', axis=0, tiled=True)]
    ppermute x0 -> x35, waiting for transfers between devices: none -> 194 us  [swap(): return lax.ppermute(value, axis, [(i, i ^ bit) for i in range(n)])]
    reduce_scatter x2 -> x0, waiting for transfers between devices: 60.2 us -> none  [the longest x1 30.7 us: local(): lax.psum_scatter(jnp.dot(picked, weight_out, preferred_element_type=jnp.f...]
    ppermute x0 -> x35, starting transfers between devices: none -> 41 us  [swap(): return lax.ppermute(value, axis, [(i, i ^ bit) for i in range(n)])]
    concatenate x0 -> x18, other arithmetic: none -> 22.8 us  [the longest x1 8.93 us: local(): jnp.concatenate([jnp.concatenate([left, left_far], axis=0), jnp.concatena...]
    dot_general x3 -> x22, matrix products: 22.6 us -> 20 us  [dot(): return jnp.dot(a, b, preferred_element_type=f32)]
  transfers between devices with their start and end apart: 8 -> 35, of which waited for: 8 -> 19; matrix products, arithmetic and copies ran while one was open for 1% -> 12% of each run, Pallas kernels for 0% -> 0%
where the time goes in v1:
time: 293 us; the launch traced here: 292 us
  waiting for transfers between devices  194 us (66%)
  starting transfers between devices  41 us (14%)
  other arithmetic  32.5 us (11%)
  matrix products  20 us (7%)
  local copies, waits for them, and re-layouts  4.13 us (1%)
    ppermute x35, waiting for transfers between devices, swap(): return lax.ppermute(value, axis, [(i, i ^ bit) for i in range(n)])  194 us
    ppermute x35, starting transfers between devices, swap(): return lax.ppermute(value, axis, [(i, i ^ bit) for i in range(n)])  41 us
    dot_general x22, matrix products, dot(): return jnp.dot(a, b, preferred_element_type=f32)  20 us
    concatenate x1, other arithmetic, local(): jnp.concatenate([jnp.concatenate([left, left_far], axis=0), jnp.concatena...  8.93 us
    concatenate x1, other arithmetic, local(): everything = jnp.concatenate([chips, swap(chips, 'tp', n_tp, 1)], axis=0)  6.12 us
  transfers between devices with their start and end apart: 35, of which 19 were waited for; matrix products, arithmetic and copies ran while one was open for 12% of the time, Pallas kernels for 0%

profile of v1, /device:TPU:0, one launch (start us, length us, event | category | flops | bytes accessed | tf_op | source)
XLA Modules:
  0.0 292.1 jit_solution(8938027031206523964)
XLA Ops:
  5.3 3.0 %collective-permute-start = (bf16[128,2048]{1,0:T(8,128)(2,1)}, bf16[128,2048]{1,0:T(8,128)(2,1)}, u32[]{:S(2)}, u32[]{:S(2)}) collective-permute-start(bf16[128,2048]{1,0:T(8,128)(2,1)} %pad_maximum_fusion.5), channel_id=1, source_target_pairs={{0,2},{1,3},{2,0},{3,1},{4,6},{5,7},{6,4},{7,5},{8,10},{9,11},{10,... | collective-permute-start | bytes 1572872 | tf_op jit(solution)/shard_map/ppermute | solution.py:84
  8.3 2.7 collective-permute-start.3
  11.0 1.6 collective-permute-start.2
  12.5 8.0 %collective-permute-done = bf16[128,2048]{1,0:T(8,128)(2,1)} collective-permute-done((bf16[128,2048]{1,0:T(8,128)(2,1)}, bf16[128,2048]{1,0:T(8,128)(2,1)}, u32[]{:S(2)}, u32[]{:S(2)}) %collective-permute-start) | collective-permute-done | bytes 524320 | tf_op jit(solution)/shard_map/ppermute | solution.py:84
  20.5 2.1 pad_maximum_fusion.1
  22.7 2.9 collective-permute-start.7
  25.6 1.6 collective-permute-start.6
  28.8 7.0 %collective-permute-done.4 = bf16[512,128]{1,0:T(8,128)(2,1)} collective-permute-done((bf16[512,128]{1,0:T(8,128)(2,1)}, bf16[512,128]{1,0:T(8,128)(2,1)}, u32[]{:S(2)}, u32[]{:S(2)}) %collective-permute-start.4) | collective-permute-done | bytes 131104 | tf_op jit(solution)/shard_map/ppermute | solution.py:84
  35.8 1.9 pad_maximum_fusion.6
  37.6 1.6 collective-permute-start.5
  40.0 1.4 collective-permute-start.8
  42.8 2.3 collective-permute-done.8
  46.6 6.1 %collective-permute-done.5 = bf16[2048,128]{1,0:T(8,128)(2,1)} collective-permute-done((bf16[2048,128]{1,0:T(8,128)(2,1)}, bf16[2048,128]{1,0:T(8,128)(2,1)}, u32[]{:S(2)}, u32[]{:S(2)}) %collective-permute-start.5) | collective-permute-done | bytes 524320 | tf_op jit(solution)/shard_map/ppermute | solution.py:84
  52.7 2.3 fusion.19
  55.5 6.7 %collective-permute-done.9 = bf16[128,2048]{1,0:T(8,128)(2,1)S(1)} collective-permute-done((bf16[128,2048]{1,0:T(8,128)(2,1)S(1)}, bf16[128,2048]{1,0:T(8,128)(2,1)S(1)}, u32[]{:S(2)}, u32[]{:S(2)}) %collective-permute-start.9) | collective-permute-done | bytes 524320 | tf_op jit(solution)/shard_map/ppermute | solution.py:84
  62.3 1.4 convolution_convert_fusion
  63.8 2.6 collective-permute-done.10
  66.4 1.4 fusion
  67.9 1.6 collective-permute-start.11
  70.7 11.2 %collective-permute-done.11 = bf16[128,2048]{1,0:T(8,128)(2,1)S(1)} collective-permute-done((bf16[128,2048]{1,0:T(8,128)(2,1)S(1)}, bf16[128,2048]{1,0:T(8,128)(2,1)S(1)}, u32[]{:S(2)}, u32[]{:S(2)}) %collective-permute-start.11) | collective-permute-done | bytes 524320 | tf_op jit(solution)/shard_map/ppermute | solution.py:84
  82.9 1.6 collective-permute-start.14
  84.6 1.6 collective-permute-start.12
  86.1 4.3 %collective-permute-done.14 = bf16[128,1024]{1,0:T(8,128)(2,1)S(1)} collective-permute-done((bf16[128,1024]{1,0:T(8,128)(2,1)S(1)}, bf16[128,1024]{1,0:T(8,128)(2,1)S(1)}, u32[]{:S(2)}, u32[]{:S(2)}) %collective-permute-start.14) | collective-permute-done | bytes 262176 | tf_op jit(solution)/shard_map/ppermute | solution.py:84
  90.5 1.6 collective-permute-start.15
  92.2 1.6 collective-permute-start.13
  93.8 9.3 %collective-permute-done.15 = bf16[256,1024]{1,0:T(8,128)(2,1)S(1)} collective-permute-done((bf16[256,1024]{1,0:T(8,128)(2,1)S(1)}, bf16[256,1024]{1,0:T(8,128)(2,1)S(1)}, u32[]{:S(2)}, u32[]{:S(2)}) %collective-permute-start.15) | collective-permute-done | bytes 524320 | tf_op jit(solution)/shard_map/ppermute | solution.py:84
  104.3 8.9 %maximum_maximum_fusion = bf16[512,2048]{1,0:T(8,128)(2,1)} fusion(bf16[128,1024]{1,0:T(8,128)(2,1)S(1)} %get-tuple-element.47, bf16[128,1024]{1,0:T(8,128)(2,1)S(1)} %collective-permute-done.14, bf16[128,1024]{1,0:T(8,128)(2,1)S(1)} %get-tuple-element.46, bf16[128,512]{1,0:T(8,128)(2,1)S(1)} %get-tuple-element.79, ...), kind=kLoop, calls=%fused_computation.17 | loop fusion | flops 18874368 | bytes 4194304 | tf_op jit(solution)/shard_map/concatenate | solution.py:160
  114.3 1.6 collective-permute-start.18
  115.9 1.5 collective-permute-start.17
  118.7 1.6 collective-permute-start.20
  120.6 43.4 %collective-permute-done.18 = bf16[512,1024]{1,0:T(8,128)(2,1)S(1)} collective-permute-done((bf16[512,1024]{1,0:T(8,128)(2,1)}, bf16[512,1024]{1,0:T(8,128)(2,1)S(1)}, u32[]{:S(2)}, u32[]{:S(2)}) %collective-permute-start.18) | collective-permute-done | bytes 1048608 | tf_op jit(solution)/shard_map/ppermute | solution.py:84
  164.0 3.1 %collective-permute-start.19 = (bf16[512,1024]{1,0:T(8,128)(2,1)S(1)}, bf16[512,1024]{1,0:T(8,128)(2,1)S(1)}, u32[]{:S(2)}, u32[]{:S(2)}) collective-permute-start(bf16[512,1024]{1,0:T(8,128)(2,1)S(1)} %collective-permute-done.18), channel_id=1, source_target_pairs={{0,4},{4,0},{8,12},{12,8},{1,5},{5,1},{9,13},{13,9},{2,6},{6,2},{1... | collective-permute-start | bytes 3145736 | tf_op jit(solution)/shard_map/ppermute | solution.py:84
  167.1 6.1 %pad_maximum_fusion = bf16[1024,2048]{1,0:T(8,128)(2,1)S(1)} fusion(bf16[512,2048]{1,0:T(8,128)(2,1)} %collective-permute-done.16, bf16[128,1024]{1,0:T(8,128)(2,1)S(1)} %copy-done.3, bf16[128,1024]{1,0:T(8,128)(2,1)S(1)} %collective-permute-done.14, bf16[128,1024]{1,0:T(8,128)(2,1)S(1)} %get-tuple-element.46, bf16[128,512]{1,0:T(8,128)(2,1)S(1)} %get-tuple-element.79, ...), kind=kLoop, calls=%fused_computation | loop fusion | flops 41943040 | bytes 8388608 | tf_op jit(solution)/shard_map/concatenate | solution.py:167
  173.2 2.5 fusion.27
  177.0 9.6 %collective-permute-done.20 = bf16[1024,256]{1,0:T(8,128)(2,1)S(1)} collective-permute-done((bf16[1024,256]{1,0:T(8,128)(2,1)S(1)}, bf16[1024,256]{1,0:T(8,128)(2,1)S(1)}, u32[]{:S(2)}, u32[]{:S(2)}) %collective-permute-start.20) | collective-permute-done | bytes 524320 | tf_op jit(solution)/shard_map/ppermute | solution.py:84
  186.6 22.0 %collective-permute-done.23 = bf16[1024,256]{1,0:T(8,128)(2,1)S(1)} collective-permute-done((bf16[1024,256]{1,0:T(8,128)(2,1)S(1)}, bf16[1024,256]{1,0:T(8,128)(2,1)S(1)}, u32[]{:S(2)}, u32[]{:S(2)}) %collective-permute-start.23) | collective-permute-done | bytes 524320 | tf_op jit(solution)/shard_map/ppermute | solution.py:84
  208.6 2.0 collective-permute-start.27
  210.6 2.5 fusion.25
  213.1 6.6 %collective-permute-done.19 = bf16[512,1024]{1,0:T(8,128)(2,1)S(1)} collective-permute-done((bf16[512,1024]{1,0:T(8,128)(2,1)S(1)}, bf16[512,1024]{1,0:T(8,128)(2,1)S(1)}, u32[]{:S(2)}, u32[]{:S(2)}) %collective-permute-start.19) | collective-permute-done | bytes 1048608 | tf_op jit(solution)/shard_map/ppermute | solution.py:84
  219.7 1.5 multiply_convert_fusion
  221.6 20.5 %collective-permute-done.21 = bf16[1024,256]{1,0:T(8,128)(2,1)S(1)} collective-permute-done((bf16[1024,256]{1,0:T(8,128)(2,1)S(1)}, bf16[1024,256]{1,0:T(8,128)(2,1)S(1)}, u32[]{:S(2)}, u32[]{:S(2)}) %collective-permute-start.21) | collective-permute-done | bytes 524320 | tf_op jit(solution)/shard_map/ppermute | solution.py:84
  243.2 10.1 %collective-permute-done.27 = bf16[1024,256]{1,0:T(8,128)(2,1)S(1)} collective-permute-done((bf16[1024,256]{1,0:T(8,128)(2,1)S(1)}, bf16[1024,256]{1,0:T(8,128)(2,1)S(1)}, u32[]{:S(2)}, u32[]{:S(2)}) %collective-permute-start.27) | collective-permute-done | bytes 524320 | tf_op jit(solution)/shard_map/ppermute | solution.py:84
  256.8 1.6 collective-permute-start.29
  262.2 1.6 collective-permute-start.33
  264.6 7.3 %collective-permute-done.25 = bf16[256,768]{1,0:T(8,128)(2,1)S(1)} collective-permute-done((bf16[256,768]{1,0:T(8,128)(2,1)S(1)}, bf16[256,768]{1,0:T(8,128)(2,1)S(1)}, u32[]{:S(2)}, u32[]{:S(2)}) %collective-permute-start.25) | collective-permute-done | bytes 393248 | tf_op jit(solution)/shard_map/ppermute | solution.py:84
  273.2 9.2 %collective-permute-done.33 = bf16[256,1024]{1,0:T(8,128)(2,1)S(1)} collective-permute-done((bf16[256,1024]{1,0:T(8,128)(2,1)S(1)}, bf16[256,1024]{1,0:T(8,128)(2,1)S(1)}, u32[]{:S(2)}, u32[]{:S(2)}) %collective-permute-start.33) | collective-permute-done | bytes 524320 | tf_op jit(solution)/shard_map/ppermute | solution.py:84
  282.7 1.3 collective-permute-start.34
  284.1 6.2 %collective-permute-done.34 = bf16[128,1024]{1,0:T(8,128)(2,1)S(1)} collective-permute-done((bf16[128,1024]{1,0:T(8,128)(2,1)S(1)}, bf16[128,1024]{1,0:T(8,128)(2,1)S(1)}, u32[]{:S(2)}, u32[]{:S(2)}) %collective-permute-start.34) | collective-permute-done | bytes 262176 | tf_op jit(solution)/shard_map/ppermute | solution.py:84
  (152 shorter events, 31.2 us)
Async XLA Ops:
  0.0 113.2 %copy-start = (bf16[512,2048]{1,0:T(8,128)(2,1)S(1)}, bf16[512,2048]{1,0:T(8,128)(2,1)}, u32[]{:S(2)}) copy-start(bf16[512,2048]{1,0:T(8,128)(2,1)} %param.11) | copy-start | bytes 6291460
  5.3 15.2 %collective-permute-start = (bf16[128,2048]{1,0:T(8,128)(2,1)}, bf16[128,2048]{1,0:T(8,128)(2,1)}, u32[]{:S(2)}, u32[]{:S(2)}) collective-permute-start(bf16[128,2048]{1,0:T(8,128)(2,1)} %pad_maximum_fusion.5), channel_id=1, source_target_pairs={{0,2},{1,3},{2,0},{3,1},{4,6},{5,7},{6,4},{7,5},{8,10},{9,11},{10,... | collective-permute-start | bytes 1572872 | tf_op jit(solution)/shard_map/ppermute | solution.py:84
  8.3 14.4 %copy-start.15 = (bf16[256,512]{1,0:T(8,128)(2,1)S(1)}, bf16[256,512]{1,0:T(8,128)(2,1)}, u32[]{:S(2)}) copy-start(bf16[256,512]{1,0:T(8,128)(2,1)} %param.10) | copy-start | bytes 786436
  8.3 18.8 %collective-permute-start.3 = (bf16[512,128]{1,0:T(8,128)(2,1)S(1)}, bf16[512,128]{1,0:T(8,128)(2,1)}, u32[]{:S(2)}, u32[]{:S(2)}) collective-permute-start(bf16[512,128]{1,0:T(8,128)(2,1)S(1)} %constant_dynamic-slice_fusion.3), channel_id=1, source_target_pairs={{0,8},{4,12},{8,0},{12,4},{1,9},{5,13},{9,1},{13,5},{2,10},{6,14},... | collective-permute-start | bytes 393224 | tf_op jit(solution)/shard_map/ppermute | solution.py:84
  11.0 17.8 %collective-permute-start.2 = (bf16[512,128]{1,0:T(8,128)(2,1)S(1)}, bf16[512,128]{1,0:T(8,128)(2,1)}, u32[]{:S(2)}, u32[]{:S(2)}) collective-permute-start(bf16[512,128]{1,0:T(8,128)(2,1)S(1)} %constant_dynamic-slice_fusion.3), channel_id=1, source_target_pairs={{0,4},{4,0},{8,12},{12,8},{1,5},{5,1},{9,13},{13,9},{2,6},{6,2},{1... | collective-permute-start | bytes 393224 | tf_op jit(solution)/shard_map/ppermute | solution.py:84
  22.6 30.1 %collective-permute-start.1 = (bf16[256,2048]{1,0:T(8,128)(2,1)}, bf16[256,2048]{1,0:T(8,128)(2,1)}, u32[]{:S(2)}, u32[]{:S(2)}) collective-permute-start(bf16[256,2048]{1,0:T(8,128)(2,1)} %pad_maximum_fusion.1), channel_id=1, source_target_pairs={{0,1},{1,0},{2,3},{3,2},{4,5},{5,4},{6,7},{7,6},{8,9},{9,8},{10,11... | collective-permute-start | bytes 3145736 | tf_op jit(solution)/shard_map/ppermute | solution.py:84
  22.7 17.4 %collective-permute-start.7 = (bf16[128,512]{1,0:T(8,128)(2,1)S(1)}, bf16[128,512]{1,0:T(8,128)(2,1)S(1)}, u32[]{:S(2)}, u32[]{:S(2)}) collective-permute-start(bf16[128,512]{1,0:T(8,128)(2,1)S(1)} %constant_dynamic-slice_fusion.2), channel_id=1, source_target_pairs={{0,8},{4,12},{8,0},{12,4},{1,9},{5,13},{9,1},{13,5},{2,10},{6,14},... | collective-permute-start | bytes 393224 | tf_op jit(solution)/shard_map/ppermute | solution.py:84
  25.6 17.2 %collective-permute-start.6 = (bf16[128,512]{1,0:T(8,128)(2,1)S(1)}, bf16[128,512]{1,0:T(8,128)(2,1)}, u32[]{:S(2)}, u32[]{:S(2)}) collective-permute-start(bf16[128,512]{1,0:T(8,128)(2,1)S(1)} %constant_dynamic-slice_fusion.2), channel_id=1, source_target_pairs={{0,4},{4,0},{8,12},{12,8},{1,5},{5,1},{9,13},{13,9},{2,6},{6,2},{1... | collective-permute-start | bytes 393224 | tf_op jit(solution)/shard_map/ppermute | solution.py:84
  27.2 8.6 %collective-permute-start.4 = (bf16[512,128]{1,0:T(8,128)(2,1)}, bf16[512,128]{1,0:T(8,128)(2,1)}, u32[]{:S(2)}, u32[]{:S(2)}) collective-permute-start(bf16[512,128]{1,0:T(8,128)(2,1)} %collective-permute-done.3), channel_id=1, source_target_pairs={{0,4},{4,0},{8,12},{12,8},{1,5},{5,1},{9,13},{13,9},{2,6},{6,2},{1... | collective-permute-start | bytes 393224 | tf_op jit(solution)/shard_map/ppermute | solution.py:84
  37.6 15.1 %collective-permute-start.5 = (bf16[2048,128]{1,0:T(8,128)(2,1)}, bf16[2048,128]{1,0:T(8,128)(2,1)}, u32[]{:S(2)}, u32[]{:S(2)}) collective-permute-start(bf16[2048,128]{1,0:T(8,128)(2,1)} %pad_maximum_fusion.6), channel_id=1, source_target_pairs={{0,16},{16,0},{1,17},{17,1},{2,18},{18,2},{3,19},{19,3},{4,20},{20... | collective-permute-start | bytes 1572872 | tf_op jit(solution)/shard_map/ppermute | solution.py:84
  40.0 5.1 %collective-permute-start.8 = (bf16[128,512]{1,0:T(8,128)(2,1)S(1)}, bf16[128,512]{1,0:T(8,128)(2,1)}, u32[]{:S(2)}, u32[]{:S(2)}) collective-permute-start(bf16[128,512]{1,0:T(8,128)(2,1)S(1)} %collective-permute-done.7), channel_id=1, source_target_pairs={{0,4},{4,0},{8,12},{12,8},{1,5},{5,1},{9,13},{13,9},{2,6},{6,2},{1... | collective-permute-start | bytes 393224 | tf_op jit(solution)/shard_map/ppermute | solution.py:84
  46.1 16.1 %collective-permute-start.9 = (bf16[128,2048]{1,0:T(8,128)(2,1)S(1)}, bf16[128,2048]{1,0:T(8,128)(2,1)S(1)}, u32[]{:S(2)}, u32[]{:S(2)}) collective-permute-start(bf16[128,2048]{1,0:T(8,128)(2,1)S(1)} %pad_maximum_fusion.7), channel_id=1, source_target_pairs={{0,16},{16,0},{1,17},{17,1},{2,18},{18,2},{3,19},{19,3},{4,20},{20... | collective-permute-start | bytes 1572872 | tf_op jit(solution)/shard_map/ppermute | solution.py:84
  63.7 2.7 collective-permute-start.10
  67.9 14.0 %collective-permute-start.11 = (bf16[128,2048]{1,0:T(8,128)(2,1)S(1)}, bf16[128,2048]{1,0:T(8,128)(2,1)S(1)}, u32[]{:S(2)}, u32[]{:S(2)}) collective-permute-start(bf16[128,2048]{1,0:T(8,128)(2,1)S(1)} %slice.371), channel_id=1, source_target_pairs={{0,2},{1,3},{2,0},{3,1},{4,6},{5,7},{6,4},{7,5},{8,10},{9,11},{10,... | collective-permute-start | bytes 1572872 | tf_op jit(solution)/shard_map/ppermute | solution.py:84
  82.7 9.5 %copy-start.6 = (bf16[128,512]{1,0:T(8,128)(2,1)}, bf16[128,512]{1,0:T(8,128)(2,1)S(1)}, u32[]{:S(2)}) copy-start(bf16[128,512]{1,0:T(8,128)(2,1)S(1)} %get-tuple-element.31) | copy-start | bytes 393220
  82.7 9.5 %copy-start.8 = (bf16[128,512]{1,0:T(8,128)(2,1)}, bf16[128,512]{1,0:T(8,128)(2,1)S(1)}, u32[]{:S(2)}) copy-start(bf16[128,512]{1,0:T(8,128)(2,1)S(1)} %get-tuple-element.35) | copy-start | bytes 393220
  82.7 9.5 %copy-start.10 = (bf16[128,512]{1,0:T(8,128)(2,1)}, bf16[128,512]{1,0:T(8,128)(2,1)S(1)}, u32[]{:S(2)}) copy-start(bf16[128,512]{1,0:T(8,128)(2,1)S(1)} %get-tuple-element.37) | copy-start | bytes 393220
  82.9 7.6 %collective-permute-start.14 = (bf16[128,1024]{1,0:T(8,128)(2,1)S(1)}, bf16[128,1024]{1,0:T(8,128)(2,1)S(1)}, u32[]{:S(2)}, u32[]{:S(2)}) collective-permute-start(bf16[128,1024]{1,0:T(8,128)(2,1)S(1)} %pad_maximum_fusion.14), channel_id=1, source_target_pairs={{0,16},{16,0},{1,17},{17,1},{2,18},{18,2},{3,19},{19,3},{4,20},{20... | collective-permute-start | bytes 786440 | tf_op jit(solution)/shard_map/ppermute | solution.py:84
  84.6 7.6 %collective-permute-start.12 = (bf16[128,1024]{1,0:T(8,128)(2,1)S(1)}, bf16[128,1024]{1,0:T(8,128)(2,1)S(1)}, u32[]{:S(2)}, u32[]{:S(2)}) collective-permute-start(bf16[128,1024]{1,0:T(8,128)(2,1)S(1)} %pad_maximum_fusion.13), channel_id=1, source_target_pairs={{0,2},{1,3},{2,0},{3,1},{4,6},{5,7},{6,4},{7,5},{8,10},{9,11},{10,... | collective-permute-start | bytes 786440 | tf_op jit(solution)/shard_map/ppermute | solution.py:84
  90.5 12.6 %collective-permute-start.15 = (bf16[256,1024]{1,0:T(8,128)(2,1)S(1)}, bf16[256,1024]{1,0:T(8,128)(2,1)S(1)}, u32[]{:S(2)}, u32[]{:S(2)}) collective-permute-start(bf16[256,1024]{1,0:T(8,128)(2,1)S(1)} %pad_maximum_fusion.9), channel_id=1, source_target_pairs={{0,2},{1,3},{2,0},{3,1},{4,6},{5,7},{6,4},{7,5},{8,10},{9,11},{10,... | collective-permute-start | bytes 1572872 | tf_op jit(solution)/shard_map/ppermute | solution.py:84
  92.2 12.0 %collective-permute-start.13 = (bf16[256,1024]{1,0:T(8,128)(2,1)S(1)}, bf16[256,1024]{1,0:T(8,128)(2,1)S(1)}, u32[]{:S(2)}, u32[]{:S(2)}) collective-permute-start(bf16[256,1024]{1,0:T(8,128)(2,1)S(1)} %pad_maximum_fusion.8), channel_id=1, source_target_pairs={{0,16},{16,0},{1,17},{17,1},{2,18},{18,2},{3,19},{19,3},{4,20},{20... | collective-permute-start | bytes 1572872 | tf_op jit(solution)/shard_map/ppermute | solution.py:84
  103.1 10.1 %copy-start.2 = (bf16[128,1024]{1,0:T(8,128)(2,1)}, bf16[128,1024]{1,0:T(8,128)(2,1)S(1)}, u32[]{:S(2)}) copy-start(bf16[128,1024]{1,0:T(8,128)(2,1)S(1)} %get-tuple-element.47) | copy-start | bytes 786436
  113.2 50.8 %collective-permute-start.16 = (bf16[512,2048]{1,0:T(8,128)(2,1)}, bf16[512,2048]{1,0:T(8,128)(2,1)}, u32[]{:S(2)}, u32[]{:S(2)}) collective-permute-start(bf16[512,2048]{1,0:T(8,128)(2,1)} %maximum_maximum_fusion), channel_id=1, source_target_pairs={{0,1},{1,0},{2,3},{3,2},{4,5},{5,4},{6,7},{7,6},{8,9},{9,8},{10,11... | collective-permute-start | bytes 6291464 | tf_op jit(solution)/shard_map/ppermute | solution.py:84
  114.3 52.8 %copy-start.3 = (bf16[128,1024]{1,0:T(8,128)(2,1)S(1)}, bf16[128,1024]{1,0:T(8,128)(2,1)}, u32[]{:S(2)}) copy-start(bf16[128,1024]{1,0:T(8,128)(2,1)} %copy-done.2) | copy-start | bytes 786436
  114.3 52.8 %copy-start.5 = (bf16[256,1024]{1,0:T(8,128)(2,1)S(1)}, bf16[256,1024]{1,0:T(8,128)(2,1)}, u32[]{:S(2)}) copy-start(bf16[256,1024]{1,0:T(8,128)(2,1)} %copy-done.4) | copy-start | bytes 1572868
  114.3 49.7 %collective-permute-start.18 = (bf16[512,1024]{1,0:T(8,128)(2,1)}, bf16[512,1024]{1,0:T(8,128)(2,1)S(1)}, u32[]{:S(2)}, u32[]{:S(2)}) collective-permute-start(bf16[512,1024]{1,0:T(8,128)(2,1)} %constant_dynamic-slice_fusion.1), channel_id=1, source_target_pairs={{0,8},{4,12},{8,0},{12,4},{1,9},{5,13},{9,1},{13,5},{2,10},{6,14},... | collective-permute-start | bytes 3145736 | tf_op jit(solution)/shard_map/ppermute | solution.py:84
  115.9 92.7 %collective-permute-start.17 = (bf16[512,1024]{1,0:T(8,128)(2,1)}, bf16[512,1024]{1,0:T(8,128)(2,1)}, u32[]{:S(2)}, u32[]{:S(2)}) collective-permute-start(bf16[512,1024]{1,0:T(8,128)(2,1)} %constant_dynamic-slice_fusion.1), channel_id=1, source_target_pairs={{0,4},{4,0},{8,12},{12,8},{1,5},{5,1},{9,13},{13,9},{2,6},{6,2},{1... | collective-permute-start | bytes 3145736 | tf_op jit(solution)/shard_map/ppermute | solution.py:84
  118.7 67.9 %collective-permute-start.20 = (bf16[1024,256]{1,0:T(8,128)(2,1)S(1)}, bf16[1024,256]{1,0:T(8,128)(2,1)S(1)}, u32[]{:S(2)}, u32[]{:S(2)}) collective-permute-start(bf16[1024,256]{1,0:T(8,128)(2,1)S(1)} %get-tuple-element.28), channel_id=1, source_target_pairs={{0,8},{4,12},{8,0},{12,4},{1,9},{5,13},{9,1},{13,5},{2,10},{6,14},... | collective-permute-start | bytes 1572872 | tf_op jit(solution)/shard_map/ppermute | solution.py:84
  120.3 134.1 %collective-permute-start.31 = (bf16[1024,256]{1,0:T(8,128)(2,1)S(1)}, bf16[1024,256]{1,0:T(8,128)(2,1)S(1)}, u32[]{:S(2)}, u32[]{:S(2)}) collective-permute-start(bf16[1024,256]{1,0:T(8,128)(2,1)S(1)} %get-tuple-element.28), channel_id=1, source_target_pairs={{0,4},{4,0},{8,12},{12,8},{1,5},{5,1},{9,13},{13,9},{2,6},{6,2},{1... | collective-permute-start | bytes 1572872 | tf_op jit(solution)/shard_map/ppermute | solution.py:84
  164.0 44.6 %collective-permute-start.23 = (bf16[1024,256]{1,0:T(8,128)(2,1)S(1)}, bf16[1024,256]{1,0:T(8,128)(2,1)S(1)}, u32[]{:S(2)}, u32[]{:S(2)}) collective-permute-start(bf16[1024,256]{1,0:T(8,128)(2,1)S(1)} %get-tuple-element.29), channel_id=1, source_target_pairs={{0,8},{4,12},{8,0},{12,4},{1,9},{5,13},{9,1},{13,5},{2,10},{6,14},... | collective-permute-start | bytes 1572872 | tf_op jit(solution)/shard_map/ppermute | solution.py:84
  164.0 55.7 %collective-permute-start.19 = (bf16[512,1024]{1,0:T(8,128)(2,1)S(1)}, bf16[512,1024]{1,0:T(8,128)(2,1)S(1)}, u32[]{:S(2)}, u32[]{:S(2)}) collective-permute-start(bf16[512,1024]{1,0:T(8,128)(2,1)S(1)} %collective-permute-done.18), channel_id=1, source_target_pairs={{0,4},{4,0},{8,12},{12,8},{1,5},{5,1},{9,13},{13,9},{2,6},{6,2},{1... | collective-permute-start | bytes 3145736 | tf_op jit(solution)/shard_map/ppermute | solution.py:84
  186.6 56.1 %collective-permute-start.22 = (bf16[1024,256]{1,0:T(8,128)(2,1)S(1)}, bf16[1024,256]{1,0:T(8,128)(2,1)S(1)}, u32[]{:S(2)}, u32[]{:S(2)}) collective-permute-start(bf16[1024,256]{1,0:T(8,128)(2,1)S(1)} %get-tuple-element.29), channel_id=1, source_target_pairs={{0,4},{4,0},{8,12},{12,8},{1,5},{5,1},{9,13},{13,9},{2,6},{6,2},{1... | collective-permute-start | bytes 1572872 | tf_op jit(solution)/shard_map/ppermute | solution.py:84
  208.6 33.6 %collective-permute-start.21 = (bf16[1024,256]{1,0:T(8,128)(2,1)S(1)}, bf16[1024,256]{1,0:T(8,128)(2,1)S(1)}, u32[]{:S(2)}, u32[]{:S(2)}) collective-permute-start(bf16[1024,256]{1,0:T(8,128)(2,1)S(1)} %collective-permute-done.20), channel_id=1, source_target_pairs={{0,4},{4,0},{8,12},{12,8},{1,5},{5,1},{9,13},{13,9},{2,6},{6,2},{1... | collective-permute-start | bytes 1572872 | tf_op jit(solution)/shard_map/ppermute | solution.py:84
  208.6 44.7 %collective-permute-start.27 = (bf16[1024,256]{1,0:T(8,128)(2,1)S(1)}, bf16[1024,256]{1,0:T(8,128)(2,1)S(1)}, u32[]{:S(2)}, u32[]{:S(2)}) collective-permute-start(bf16[1024,256]{1,0:T(8,128)(2,1)S(1)} %collective-permute-done.23), channel_id=1, source_target_pairs={{0,4},{4,0},{8,12},{12,8},{1,5},{5,1},{9,13},{13,9},{2,6},{6,2},{1... | collective-permute-start | bytes 1572872 | tf_op jit(solution)/shard_map/ppermute | solution.py:84
  243.1 15.3 %collective-permute-start.24 = (bf16[512,768]{1,0:T(8,128)(2,1)S(1)}, bf16[512,768]{1,0:T(8,128)(2,1)S(1)}, u32[]{:S(2)}, u32[]{:S(2)}) collective-permute-start(bf16[512,768]{1,0:T(8,128)(2,1)S(1)} %pad_maximum_fusion.4), channel_id=1, source_target_pairs={{0,1},{1,0},{2,3},{3,2},{4,5},{5,4},{6,7},{7,6},{8,9},{9,8},{10,11... | collective-permute-start | bytes 2359304 | tf_op jit(solution)/shard_map/ppermute | solution.py:84
  253.8 2.6 collective-permute-start.28
  256.2 4.2 %collective-permute-start.32 = (bf16[512,1024]{1,0:T(8,128)(2,1)S(1)}, bf16[512,1024]{1,0:T(8,128)(2,1)S(1)}, u32[]{:S(2)}, u32[]{:S(2)}) collective-permute-start(bf16[512,1024]{1,0:T(8,128)(2,1)S(1)} %pad_maximum_fusion.3), channel_id=1, source_target_pairs={{0,1},{1,0},{2,3},{3,2},{4,5},{5,4},{6,7},{7,6},{8,9},{9,8},{10,11... | collective-permute-start | bytes 3145736 | tf_op jit(solution)/shard_map/ppermute | solution.py:84
  256.8 6.9 %collective-permute-start.29 = (bf16[256,256]{1,0:T(8,128)(2,1)S(1)}, bf16[256,256]{1,0:T(8,128)(2,1)S(1)}, u32[]{:S(2)}, u32[]{:S(2)}) collective-permute-start(bf16[256,256]{1,0:T(8,128)(2,1)S(1)} %slice.402), channel_id=1, source_target_pairs={{0,16},{16,0},{1,17},{17,1},{2,18},{18,2},{3,19},{19,3},{4,20},{20... | collective-permute-start | bytes 393224 | tf_op jit(solution)/shard_map/ppermute | solution.py:84
  259.8 12.1 %collective-permute-start.25 = (bf16[256,768]{1,0:T(8,128)(2,1)S(1)}, bf16[256,768]{1,0:T(8,128)(2,1)S(1)}, u32[]{:S(2)}, u32[]{:S(2)}) collective-permute-start(bf16[256,768]{1,0:T(8,128)(2,1)S(1)} %pad_maximum_fusion.12), channel_id=1, source_target_pairs={{0,16},{16,0},{1,17},{17,1},{2,18},{18,2},{3,19},{19,3},{4,20},{20... | collective-permute-start | bytes 1179656 | tf_op jit(solution)/shard_map/ppermute | solution.py:84
  262.2 20.3 %collective-permute-start.33 = (bf16[256,1024]{1,0:T(8,128)(2,1)S(1)}, bf16[256,1024]{1,0:T(8,128)(2,1)S(1)}, u32[]{:S(2)}, u32[]{:S(2)}) collective-permute-start(bf16[256,1024]{1,0:T(8,128)(2,1)S(1)} %pad_maximum_fusion.10), channel_id=1, source_target_pairs={{0,16},{16,0},{1,17},{17,1},{2,18},{18,2},{3,19},{19,3},{4,20},{20... | collective-permute-start | bytes 1572872 | tf_op jit(solution)/shard_map/ppermute | solution.py:84
  263.8 20.1 %collective-permute-start.30 = (bf16[128,256]{1,0:T(8,128)(2,1)S(1)}, bf16[128,256]{1,0:T(8,128)(2,1)S(1)}, u32[]{:S(2)}, u32[]{:S(2)}) collective-permute-start(bf16[128,256]{1,0:T(8,128)(2,1)S(1)} %slice.404), channel_id=1, source_target_pairs={{0,2},{1,3},{2,0},{3,1},{4,6},{5,7},{6,4},{7,5},{8,10},{9,11},{10,... | collective-permute-start | bytes 196616 | tf_op jit(solution)/shard_map/ppermute | solution.py:84
  272.1 18.7 %copy-start.7 = (bf16[128,512]{1,0:T(8,128)(2,1)S(1)}, bf16[128,512]{1,0:T(8,128)(2,1)}, u32[]{:S(2)}) copy-start(bf16[128,512]{1,0:T(8,128)(2,1)} %copy-done.6) | copy-start | bytes 393220
  272.1 18.7 %copy-start.9 = (bf16[128,512]{1,0:T(8,128)(2,1)S(1)}, bf16[128,512]{1,0:T(8,128)(2,1)}, u32[]{:S(2)}) copy-start(bf16[128,512]{1,0:T(8,128)(2,1)} %copy-done.8) | copy-start | bytes 393220
  272.1 18.7 %copy-start.11 = (bf16[128,512]{1,0:T(8,128)(2,1)S(1)}, bf16[128,512]{1,0:T(8,128)(2,1)}, u32[]{:S(2)}) copy-start(bf16[128,512]{1,0:T(8,128)(2,1)} %copy-done.10) | copy-start | bytes 393220
  272.1 18.7 %copy-start.16 = (f32[1,512]{1,0:T(1,128)S(1)}, f32[1,512]{1,0:T(1,128)}, u32[]{:S(2)}) copy-start(f32[1,512]{1,0:T(1,128)} %get-tuple-element.60) | copy-start | bytes 6148
  272.1 18.7 %copy-start.17 = (f32[1,512]{1,0:T(1,128)S(1)}, f32[1,512]{1,0:T(1,128)}, u32[]{:S(2)}) copy-start(f32[1,512]{1,0:T(1,128)} %get-tuple-element.64) | copy-start | bytes 6148
  272.1 11.9 %collective-permute-start.26 = (bf16[128,768]{1,0:T(8,128)(2,1)S(1)}, bf16[128,768]{1,0:T(8,128)(2,1)S(1)}, u32[]{:S(2)}, u32[]{:S(2)}) collective-permute-start(bf16[128,768]{1,0:T(8,128)(2,1)S(1)} %pad_maximum_fusion.16), channel_id=1, source_target_pairs={{0,2},{1,3},{2,0},{3,1},{4,6},{5,7},{6,4},{7,5},{8,10},{9,11},{10,... | collective-permute-start | bytes 589832 | tf_op jit(solution)/shard_map/ppermute | solution.py:84
  282.7 7.7 %collective-permute-start.34 = (bf16[128,1024]{1,0:T(8,128)(2,1)S(1)}, bf16[128,1024]{1,0:T(8,128)(2,1)S(1)}, u32[]{:S(2)}, u32[]{:S(2)}) collective-permute-start(bf16[128,1024]{1,0:T(8,128)(2,1)S(1)} %pad_maximum_fusion.15), channel_id=1, source_target_pairs={{0,2},{1,3},{2,0},{3,1},{4,6},{5,7},{6,4},{7,5},{8,10},{9,11},{10,... | collective-permute-start | bytes 786440 | tf_op jit(solution)/shard_map/ppermute | solution.py:84
  (6 other events, 35.2 us)

commit v2 on v1

--- a/solution.py
+++ b/solution.py
@@ -75,6 +75,10 @@
     return lax.rsqrt(total / width + norm_eps)
 
 
+def tie(value, *after):
+    return lax.optimization_barrier((value,) + after)[0] if after else value
+
+
 def dot(a, b):
     return jnp.dot(a, b, preferred_element_type=f32)
 
@@ -100,12 +104,16 @@
         def gather_fs(value):
             two = swap(value, "fs", n_fs, 2)
             one = swap(value, "fs", n_fs, 1)
-            three = swap(two, "fs", n_fs, 1)
-            return [value, one, two, three]
+            return [value, one, two]
+
+        def last_hop(pieces, *after):
+            pieces.append(swap(tie(pieces[2], *after), "fs", n_fs, 1))
 
         mi = gather_fs(lax.dynamic_slice_in_dim(mix_in, g * part, part, axis=1))
         mo = gather_fs(lax.dynamic_slice_in_dim(mix_out, g * part, part, axis=0))
         up = gather_fs(lax.dynamic_slice_in_dim(up, g * ff, ff, axis=1))
+        for pieces in (mi, mo, up):
+            last_hop(pieces)
         down = lax.dynamic_slice_in_dim(down, g * ff, ff, axis=0)
         down_a = gather_fs(down[:, :col // 2])
         down_b = gather_fs(down[:, col // 2:])
@@ -181,17 +189,22 @@
             total = [(dot(squared[:half], w) + got[:, a:b].astype(f32)).astype(bf16) for w, (a, b) in zip(weights, spans)]
             got = swap(jnp.concatenate([v[half // 2:] for v in total], axis=1), "grp", n_grp, 1)
             total = [(v[:half // 2].astype(f32) + got[:, a:b].astype(f32)).astype(bf16) for v, (a, b) in zip(total, spans)]
+            stage.append(total[0])
             got = swap(jnp.concatenate([v[rows:] for v in total], axis=1), "tp", n_tp, 2)
             return [(v[:rows].astype(f32) + got[:, a:b].astype(f32)).astype(bf16) for v, (a, b) in zip(total, spans)]
 
+        stage = []
+        last_hop(down_a, squared)
+        last_hop(down_b, squared)
         first = add_up([down, down_a[1], down_a[2]])
-        second = add_up([down_b[1], down_b[2], down_a[3]])
-        third = add_up([down_b[3]])
+        second = add_up([tie(v, stage[0]) for v in down_b[1:3]])
+        third = add_up([tie(down_a[3], stage[1])])
+        fourth = add_up([tie(down_b[3], stage[2])])
         channel_out = [
             first[0],
             jnp.concatenate([first[1], second[0]], axis=1),
             jnp.concatenate([first[2], second[1]], axis=1),
-            jnp.concatenate([second[2], third[0]], axis=1),
+            jnp.concatenate([third[0], fourth[0]], axis=1),
         ]
         r = rsqrt_mean(channel_out, width)
         result = [(middle[j].astype(f32) + channel_out[j].astype(f32) * r * gain[3][j]).astype(bf16) for j in range(n_fs)]

time: 293 us -> 288 us (0.983)
  waiting for transfers between devices: 194 us -> 190 us
    ppermute x35 -> x38, waiting for transfers between devices: 194 us -> 190 us  [swap(): return lax.ppermute(value, axis, [(i, i ^ bit) for i in range(n)])]
    ppermute x35 -> x38, starting transfers between devices: 41 us -> 40.7 us  [swap(): return lax.ppermute(value, axis, [(i, i ^ bit) for i in range(n)])]
  transfers between devices with their start and end apart: 35 -> 38, of which waited for: 19 -> 27; matrix products, arithmetic and copies ran while one was open for 12% -> 12% of each run, Pallas kernels for 0% -> 0%
where the time goes in v2:
time: 288 us
  waiting for transfers between devices  190 us (66%)
  starting transfers between devices  40.7 us (14%)
  other arithmetic  32.4 us (11%)
  matrix products  20 us (7%)
  local copies, waits for them, and re-layouts  3.49 us (1%)
    ppermute x38, waiting for transfers between devices, swap(): return lax.ppermute(value, axis, [(i, i ^ bit) for i in range(n)])  190 us
    ppermute x38, starting transfers between devices, swap(): return lax.ppermute(value, axis, [(i, i ^ bit) for i in range(n)])  40.7 us
    dot_general x22, matrix products, dot(): return jnp.dot(a, b, preferred_element_type=f32)  20 us
    concatenate x1, other arithmetic, local(): jnp.concatenate([jnp.concatenate([left, left_far], axis=0), jnp.concatena...  8.95 us
    concatenate x1, other arithmetic, local(): everything = jnp.concatenate([chips, swap(chips, 'tp', n_tp, 1)], axis=0)  6.13 us
  transfers between devices with their start and end apart: 38, of which 27 were waited for; matrix products, arithmetic and copies ran while one was open for 12% of the time, Pallas kernels for 0%

profile of v2, /device:TPU:0, one launch (start us, length us, event | category | flops | bytes accessed | tf_op | source)
XLA Modules:
  0.0 287.8 jit_solution(15331883302668458811)
XLA Ops:
  5.3 3.0 %collective-permute-start = (bf16[128,2048]{1,0:T(8,128)(2,1)}, bf16[128,2048]{1,0:T(8,128)(2,1)}, u32[]{:S(2)}, u32[]{:S(2)}) collective-permute-start(bf16[128,2048]{1,0:T(8,128)(2,1)} %pad_maximum_fusion.4), channel_id=1, source_target_pairs={{0,2},{1,3},{2,0},{3,1},{4,6},{5,7},{6,4},{7,5},{8,10},{9,11},{10,... | collective-permute-start | bytes 1572872 | tf_op jit(solution)/shard_map/ppermute | solution.py:88
  8.3 2.7 collective-permute-start.3
  11.0 1.6 collective-permute-start.2
  12.5 8.0 %collective-permute-done = bf16[128,2048]{1,0:T(8,128)(2,1)} collective-permute-done((bf16[128,2048]{1,0:T(8,128)(2,1)}, bf16[128,2048]{1,0:T(8,128)(2,1)}, u32[]{:S(2)}, u32[]{:S(2)}) %collective-permute-start) | collective-permute-done | bytes 524320 | tf_op jit(solution)/shard_map/ppermute | solution.py:88
  20.5 2.1 pad_maximum_fusion.1
  22.7 2.9 %collective-permute-start.7 = (bf16[128,512]{1,0:T(8,128)(2,1)S(1)}, bf16[128,512]{1,0:T(8,128)(2,1)S(1)}, u32[]{:S(2)}, u32[]{:S(2)}) collective-permute-start(bf16[128,512]{1,0:T(8,128)(2,1)S(1)} %constant_dynamic-slice_fusion.2), channel_id=1, source_target_pairs={{0,8},{4,12},{8,0},{12,4},{1,9},{5,13},{9,1},{13,5},{2,10},{6,14},... | collective-permute-start | bytes 393224 | tf_op jit(solution)/shard_map/ppermute | solution.py:88
  25.6 1.6 collective-permute-start.6
  28.8 7.0 %collective-permute-done.4 = bf16[512,128]{1,0:T(8,128)(2,1)} collective-permute-done((bf16[512,128]{1,0:T(8,128)(2,1)}, bf16[512,128]{1,0:T(8,128)(2,1)}, u32[]{:S(2)}, u32[]{:S(2)}) %collective-permute-start.4) | collective-permute-done | bytes 131104 | tf_op jit(solution)/shard_map/ppermute | solution.py:88
  35.8 1.9 pad_maximum_fusion.5
  37.6 1.6 collective-permute-start.5
  40.0 1.4 collective-permute-start.8
  42.8 2.3 collective-permute-done.8
  46.7 6.1 %collective-permute-done.5 = bf16[2048,128]{1,0:T(8,128)(2,1)} collective-permute-done((bf16[2048,128]{1,0:T(8,128)(2,1)}, bf16[2048,128]{1,0:T(8,128)(2,1)}, u32[]{:S(2)}, u32[]{:S(2)}) %collective-permute-start.5) | collective-permute-done | bytes 524320 | tf_op jit(solution)/shard_map/ppermute | solution.py:88
  52.8 2.3 fusion.19
  55.6 6.7 %collective-permute-done.9 = bf16[128,2048]{1,0:T(8,128)(2,1)S(1)} collective-permute-done((bf16[128,2048]{1,0:T(8,128)(2,1)S(1)}, bf16[128,2048]{1,0:T(8,128)(2,1)S(1)}, u32[]{:S(2)}, u32[]{:S(2)}) %collective-permute-start.9) | collective-permute-done | bytes 524320 | tf_op jit(solution)/shard_map/ppermute | solution.py:88
  62.3 1.4 convolution_convert_fusion
  63.8 2.6 collective-permute-done.10
  66.4 1.4 fusion
  67.9 1.6 collective-permute-start.11
  70.7 11.2 %collective-permute-done.11 = bf16[128,2048]{1,0:T(8,128)(2,1)S(1)} collective-permute-done((bf16[128,2048]{1,0:T(8,128)(2,1)S(1)}, bf16[128,2048]{1,0:T(8,128)(2,1)S(1)}, u32[]{:S(2)}, u32[]{:S(2)}) %collective-permute-start.11) | collective-permute-done | bytes 524320 | tf_op jit(solution)/shard_map/ppermute | solution.py:88
  83.0 1.6 collective-permute-start.14
  84.6 1.6 collective-permute-start.12
  86.2 4.3 %collective-permute-done.14 = bf16[128,1024]{1,0:T(8,128)(2,1)S(1)} collective-permute-done((bf16[128,1024]{1,0:T(8,128)(2,1)S(1)}, bf16[128,1024]{1,0:T(8,128)(2,1)S(1)}, u32[]{:S(2)}, u32[]{:S(2)}) %collective-permute-start.14) | collective-permute-done | bytes 262176 | tf_op jit(solution)/shard_map/ppermute | solution.py:88
  90.6 1.6 collective-permute-start.15
  92.2 1.6 collective-permute-start.13
  93.8 9.3 %collective-permute-done.15 = bf16[256,1024]{1,0:T(8,128)(2,1)S(1)} collective-permute-done((bf16[256,1024]{1,0:T(8,128)(2,1)S(1)}, bf16[256,1024]{1,0:T(8,128)(2,1)S(1)}, u32[]{:S(2)}, u32[]{:S(2)}) %collective-permute-start.15) | collective-permute-done | bytes 524320 | tf_op jit(solution)/shard_map/ppermute | solution.py:88
  104.3 9.0 %maximum_maximum_fusion = bf16[512,2048]{1,0:T(8,128)(2,1)} fusion(bf16[128,1024]{1,0:T(8,128)(2,1)S(1)} %get-tuple-element.59, bf16[128,1024]{1,0:T(8,128)(2,1)S(1)} %collective-permute-done.14, bf16[128,1024]{1,0:T(8,128)(2,1)S(1)} %get-tuple-element.58, bf16[128,512]{1,0:T(8,128)(2,1)S(1)} %get-tuple-element.89, ...), kind=kLoop, calls=%fused_computation.17 | loop fusion | flops 18874368 | bytes 4194304 | tf_op jit(solution)/shard_map/concatenate | solution.py:168
  114.4 1.6 collective-permute-start.18
  116.0 1.5 collective-permute-start.17
  118.7 1.6 collective-permute-start.20
  120.7 43.4 %collective-permute-done.18 = bf16[512,1024]{1,0:T(8,128)(2,1)S(1)} collective-permute-done((bf16[512,1024]{1,0:T(8,128)(2,1)}, bf16[512,1024]{1,0:T(8,128)(2,1)S(1)}, u32[]{:S(2)}, u32[]{:S(2)}) %collective-permute-start.18) | collective-permute-done | bytes 1048608 | tf_op jit(solution)/shard_map/ppermute | solution.py:88
  164.1 6.1 %pad_maximum_fusion = bf16[1024,2048]{1,0:T(8,128)(2,1)S(1)} fusion(bf16[512,2048]{1,0:T(8,128)(2,1)} %collective-permute-done.16, bf16[128,1024]{1,0:T(8,128)(2,1)S(1)} %copy-done.3, bf16[128,1024]{1,0:T(8,128)(2,1)S(1)} %collective-permute-done.14, bf16[128,1024]{1,0:T(8,128)(2,1)S(1)} %get-tuple-element.58, bf16[128,512]{1,0:T(8,128)(2,1)S(1)} %get-tuple-element.89, ...), kind=kLoop, calls=%fused_computation | loop fusion | flops 41943040 | bytes 8388608 | tf_op jit(solution)/shard_map/concatenate | solution.py:175
  170.2 2.5 fusion.27
  174.0 2.5 fusion.25
  176.5 32.0 %collective-permute-done.19 = bf16[512,1024]{1,0:T(8,128)(2,1)S(1)} collective-permute-done((bf16[512,1024]{1,0:T(8,128)(2,1)S(1)}, bf16[512,1024]{1,0:T(8,128)(2,1)S(1)}, u32[]{:S(2)}, u32[]{:S(2)}) %collective-permute-start.19) | collective-permute-done | bytes 1048608 | tf_op jit(solution)/shard_map/ppermute | solution.py:88
  208.4 1.5 multiply_convert_fusion
  211.8 2.6 collective-permute-done.24
  216.2 1.6 collective-permute-start.25
  218.5 2.5 collective-permute-start.26
  221.1 9.1 %collective-permute-done.25 = bf16[256,1024]{1,0:T(8,128)(2,1)S(1)} collective-permute-done((bf16[256,1024]{1,0:T(8,128)(2,1)S(1)}, bf16[256,1024]{1,0:T(8,128)(2,1)S(1)}, u32[]{:S(2)}, u32[]{:S(2)}) %collective-permute-start.25) | collective-permute-done | bytes 524320 | tf_op jit(solution)/shard_map/ppermute | solution.py:88
  230.3 12.3 %collective-permute-done.22 = bf16[1024,256]{1,0:T(8,128)(2,1)S(1)} collective-permute-done((bf16[1024,256]{1,0:T(8,128)(2,1)S(1)}, bf16[1024,256]{1,0:T(8,128)(2,1)S(1)}, u32[]{:S(2)}, u32[]{:S(2)}) %collective-permute-start.22) | collective-permute-done | bytes 524320 | tf_op jit(solution)/shard_map/ppermute | solution.py:88
  245.2 1.4 collective-permute-done.27
  248.1 7.8 %collective-permute-done.28 = bf16[256,512]{1,0:T(8,128)(2,1)S(1)} collective-permute-done((bf16[256,512]{1,0:T(8,128)(2,1)S(1)}, bf16[256,512]{1,0:T(8,128)(2,1)S(1)}, u32[]{:S(2)}, u32[]{:S(2)}) %collective-permute-start.28) | collective-permute-done | bytes 262176 | tf_op jit(solution)/shard_map/ppermute | solution.py:88
  256.0 3.0 %collective-permute-done.21 = bf16[1024,256]{1,0:T(8,128)(2,1)S(1)} collective-permute-done((bf16[1024,256]{1,0:T(8,128)(2,1)S(1)}, bf16[1024,256]{1,0:T(8,128)(2,1)S(1)}, u32[]{:S(2)}, u32[]{:S(2)}) %collective-permute-start.21) | collective-permute-done | bytes 524320 | tf_op jit(solution)/shard_map/ppermute | solution.py:88
  263.5 3.6 %collective-permute-done.30 = bf16[256,256]{1,0:T(8,128)(2,1)S(1)} collective-permute-done((bf16[256,256]{1,0:T(8,128)(2,1)S(1)}, bf16[256,256]{1,0:T(8,128)(2,1)S(1)}, u32[]{:S(2)}, u32[]{:S(2)}) %collective-permute-start.30) | collective-permute-done | bytes 131104 | tf_op jit(solution)/shard_map/ppermute | solution.py:88
  267.2 6.7 %collective-permute-done.32 = bf16[1024,256]{1,0:T(8,128)(2,1)S(1)} collective-permute-done((bf16[1024,256]{1,0:T(8,128)(2,1)S(1)}, bf16[1024,256]{1,0:T(8,128)(2,1)S(1)}, u32[]{:S(2)}, u32[]{:S(2)}) %collective-permute-start.32) | collective-permute-done | bytes 524320 | tf_op jit(solution)/shard_map/ppermute | solution.py:88
  277.0 3.6 %collective-permute-done.37 = bf16[128,512]{1,0:T(8,128)(2,1)S(1)} collective-permute-done((bf16[128,512]{1,0:T(8,128)(2,1)S(1)}, bf16[128,512]{1,0:T(8,128)(2,1)S(1)}, u32[]{:S(2)}, u32[]{:S(2)}) %collective-permute-start.37) | collective-permute-done | bytes 131104 | tf_op jit(solution)/shard_map/ppermute | solution.py:88
  283.1 2.3 collective-permute-done.31
  (160 shorter events, 39.4 us)
Async XLA Ops:
  0.0 113.3 %copy-start = (bf16[512,2048]{1,0:T(8,128)(2,1)S(1)}, bf16[512,2048]{1,0:T(8,128)(2,1)}, u32[]{:S(2)}) copy-start(bf16[512,2048]{1,0:T(8,128)(2,1)} %param.11) | copy-start | bytes 6291460
  5.3 15.2 %collective-permute-start = (bf16[128,2048]{1,0:T(8,128)(2,1)}, bf16[128,2048]{1,0:T(8,128)(2,1)}, u32[]{:S(2)}, u32[]{:S(2)}) collective-permute-start(bf16[128,2048]{1,0:T(8,128)(2,1)} %pad_maximum_fusion.4), channel_id=1, source_target_pairs={{0,2},{1,3},{2,0},{3,1},{4,6},{5,7},{6,4},{7,5},{8,10},{9,11},{10,... | collective-permute-start | bytes 1572872 | tf_op jit(solution)/shard_map/ppermute | solution.py:88
  8.3 14.4 %copy-start.15 = (bf16[256,512]{1,0:T(8,128)(2,1)S(1)}, bf16[256,512]{1,0:T(8,128)(2,1)}, u32[]{:S(2)}) copy-start(bf16[256,512]{1,0:T(8,128)(2,1)} %param.10) | copy-start | bytes 786436
  8.3 18.9 %collective-permute-start.3 = (bf16[512,128]{1,0:T(8,128)(2,1)S(1)}, bf16[512,128]{1,0:T(8,128)(2,1)}, u32[]{:S(2)}, u32[]{:S(2)}) collective-permute-start(bf16[512,128]{1,0:T(8,128)(2,1)S(1)} %constant_dynamic-slice_fusion.3), channel_id=1, source_target_pairs={{0,8},{4,12},{8,0},{12,4},{1,9},{5,13},{9,1},{13,5},{2,10},{6,14},... | collective-permute-start | bytes 393224 | tf_op jit(solution)/shard_map/ppermute | solution.py:88
  11.0 17.8 %collective-permute-start.2 = (bf16[512,128]{1,0:T(8,128)(2,1)S(1)}, bf16[512,128]{1,0:T(8,128)(2,1)}, u32[]{:S(2)}, u32[]{:S(2)}) collective-permute-start(bf16[512,128]{1,0:T(8,128)(2,1)S(1)} %constant_dynamic-slice_fusion.3), channel_id=1, source_target_pairs={{0,4},{4,0},{8,12},{12,8},{1,5},{5,1},{9,13},{13,9},{2,6},{6,2},{1... | collective-permute-start | bytes 393224 | tf_op jit(solution)/shard_map/ppermute | solution.py:88
  22.7 30.1 %collective-permute-start.1 = (bf16[256,2048]{1,0:T(8,128)(2,1)}, bf16[256,2048]{1,0:T(8,128)(2,1)}, u32[]{:S(2)}, u32[]{:S(2)}) collective-permute-start(bf16[256,2048]{1,0:T(8,128)(2,1)} %pad_maximum_fusion.1), channel_id=1, source_target_pairs={{0,1},{1,0},{2,3},{3,2},{4,5},{5,4},{6,7},{7,6},{8,9},{9,8},{10,11... | collective-permute-start | bytes 3145736 | tf_op jit(solution)/shard_map/ppermute | solution.py:88
  22.7 17.4 %collective-permute-start.7 = (bf16[128,512]{1,0:T(8,128)(2,1)S(1)}, bf16[128,512]{1,0:T(8,128)(2,1)S(1)}, u32[]{:S(2)}, u32[]{:S(2)}) collective-permute-start(bf16[128,512]{1,0:T(8,128)(2,1)S(1)} %constant_dynamic-slice_fusion.2), channel_id=1, source_target_pairs={{0,8},{4,12},{8,0},{12,4},{1,9},{5,13},{9,1},{13,5},{2,10},{6,14},... | collective-permute-start | bytes 393224 | tf_op jit(solution)/shard_map/ppermute | solution.py:88
  25.6 17.2 %collective-permute-start.6 = (bf16[128,512]{1,0:T(8,128)(2,1)S(1)}, bf16[128,512]{1,0:T(8,128)(2,1)}, u32[]{:S(2)}, u32[]{:S(2)}) collective-permute-start(bf16[128,512]{1,0:T(8,128)(2,1)S(1)} %constant_dynamic-slice_fusion.2), channel_id=1, source_target_pairs={{0,4},{4,0},{8,12},{12,8},{1,5},{5,1},{9,13},{13,9},{2,6},{6,2},{1... | collective-permute-start | bytes 393224 | tf_op jit(solution)/shard_map/ppermute | solution.py:88
  27.2 8.6 %collective-permute-start.4 = (bf16[512,128]{1,0:T(8,128)(2,1)}, bf16[512,128]{1,0:T(8,128)(2,1)}, u32[]{:S(2)}, u32[]{:S(2)}) collective-permute-start(bf16[512,128]{1,0:T(8,128)(2,1)} %collective-permute-done.3), channel_id=1, source_target_pairs={{0,4},{4,0},{8,12},{12,8},{1,5},{5,1},{9,13},{13,9},{2,6},{6,2},{1... | collective-permute-start | bytes 393224 | tf_op jit(solution)/shard_map/ppermute | solution.py:88
  37.6 15.1 %collective-permute-start.5 = (bf16[2048,128]{1,0:T(8,128)(2,1)}, bf16[2048,128]{1,0:T(8,128)(2,1)}, u32[]{:S(2)}, u32[]{:S(2)}) collective-permute-start(bf16[2048,128]{1,0:T(8,128)(2,1)} %pad_maximum_fusion.5), channel_id=1, source_target_pairs={{0,16},{16,0},{1,17},{17,1},{2,18},{18,2},{3,19},{19,3},{4,20},{20... | collective-permute-start | bytes 1572872 | tf_op jit(solution)/shard_map/ppermute | solution.py:88
  40.0 5.1 %collective-permute-start.8 = (bf16[128,512]{1,0:T(8,128)(2,1)S(1)}, bf16[128,512]{1,0:T(8,128)(2,1)}, u32[]{:S(2)}, u32[]{:S(2)}) collective-permute-start(bf16[128,512]{1,0:T(8,128)(2,1)S(1)} %collective-permute-done.7), channel_id=1, source_target_pairs={{0,4},{4,0},{8,12},{12,8},{1,5},{5,1},{9,13},{13,9},{2,6},{6,2},{1... | collective-permute-start | bytes 393224 | tf_op jit(solution)/shard_map/ppermute | solution.py:88
  46.1 16.1 %collective-permute-start.9 = (bf16[128,2048]{1,0:T(8,128)(2,1)S(1)}, bf16[128,2048]{1,0:T(8,128)(2,1)S(1)}, u32[]{:S(2)}, u32[]{:S(2)}) collective-permute-start(bf16[128,2048]{1,0:T(8,128)(2,1)S(1)} %pad_maximum_fusion.6), channel_id=1, source_target_pairs={{0,16},{16,0},{1,17},{17,1},{2,18},{18,2},{3,19},{19,3},{4,20},{20... | collective-permute-start | bytes 1572872 | tf_op jit(solution)/shard_map/ppermute | solution.py:88
  63.7 2.7 collective-permute-start.10
  67.9 14.0 %collective-permute-start.11 = (bf16[128,2048]{1,0:T(8,128)(2,1)S(1)}, bf16[128,2048]{1,0:T(8,128)(2,1)S(1)}, u32[]{:S(2)}, u32[]{:S(2)}) collective-permute-start(bf16[128,2048]{1,0:T(8,128)(2,1)S(1)} %slice.359), channel_id=1, source_target_pairs={{0,2},{1,3},{2,0},{3,1},{4,6},{5,7},{6,4},{7,5},{8,10},{9,11},{10,... | collective-permute-start | bytes 1572872 | tf_op jit(solution)/shard_map/ppermute | solution.py:88
  83.0 7.6 %collective-permute-start.14 = (bf16[128,1024]{1,0:T(8,128)(2,1)S(1)}, bf16[128,1024]{1,0:T(8,128)(2,1)S(1)}, u32[]{:S(2)}, u32[]{:S(2)}) collective-permute-start(bf16[128,1024]{1,0:T(8,128)(2,1)S(1)} %pad_maximum_fusion.13), channel_id=1, source_target_pairs={{0,16},{16,0},{1,17},{17,1},{2,18},{18,2},{3,19},{19,3},{4,20},{20... | collective-permute-start | bytes 786440 | tf_op jit(solution)/shard_map/ppermute | solution.py:88
  84.6 7.6 %collective-permute-start.12 = (bf16[128,1024]{1,0:T(8,128)(2,1)S(1)}, bf16[128,1024]{1,0:T(8,128)(2,1)S(1)}, u32[]{:S(2)}, u32[]{:S(2)}) collective-permute-start(bf16[128,1024]{1,0:T(8,128)(2,1)S(1)} %pad_maximum_fusion.12), channel_id=1, source_target_pairs={{0,2},{1,3},{2,0},{3,1},{4,6},{5,7},{6,4},{7,5},{8,10},{9,11},{10,... | collective-permute-start | bytes 786440 | tf_op jit(solution)/shard_map/ppermute | solution.py:88
  90.6 12.6 %collective-permute-start.15 = (bf16[256,1024]{1,0:T(8,128)(2,1)S(1)}, bf16[256,1024]{1,0:T(8,128)(2,1)S(1)}, u32[]{:S(2)}, u32[]{:S(2)}) collective-permute-start(bf16[256,1024]{1,0:T(8,128)(2,1)S(1)} %pad_maximum_fusion.8), channel_id=1, source_target_pairs={{0,2},{1,3},{2,0},{3,1},{4,6},{5,7},{6,4},{7,5},{8,10},{9,11},{10,... | collective-permute-start | bytes 1572872 | tf_op jit(solution)/shard_map/ppermute | solution.py:88
  92.2 12.0 %collective-permute-start.13 = (bf16[256,1024]{1,0:T(8,128)(2,1)S(1)}, bf16[256,1024]{1,0:T(8,128)(2,1)S(1)}, u32[]{:S(2)}, u32[]{:S(2)}) collective-permute-start(bf16[256,1024]{1,0:T(8,128)(2,1)S(1)} %pad_maximum_fusion.7), channel_id=1, source_target_pairs={{0,16},{16,0},{1,17},{17,1},{2,18},{18,2},{3,19},{19,3},{4,20},{20... | collective-permute-start | bytes 1572872 | tf_op jit(solution)/shard_map/ppermute | solution.py:88
  113.2 50.8 %collective-permute-start.16 = (bf16[512,2048]{1,0:T(8,128)(2,1)}, bf16[512,2048]{1,0:T(8,128)(2,1)}, u32[]{:S(2)}, u32[]{:S(2)}) collective-permute-start(bf16[512,2048]{1,0:T(8,128)(2,1)} %maximum_maximum_fusion), channel_id=1, source_target_pairs={{0,1},{1,0},{2,3},{3,2},{4,5},{5,4},{6,7},{7,6},{8,9},{9,8},{10,11... | collective-permute-start | bytes 6291464 | tf_op jit(solution)/shard_map/ppermute | solution.py:88
  114.4 49.7 %copy-start.3 = (bf16[128,1024]{1,0:T(8,128)(2,1)S(1)}, bf16[128,1024]{1,0:T(8,128)(2,1)}, u32[]{:S(2)}) copy-start(bf16[128,1024]{1,0:T(8,128)(2,1)} %copy-done.2) | copy-start | bytes 786436
  114.4 49.7 %copy-start.5 = (bf16[256,1024]{1,0:T(8,128)(2,1)S(1)}, bf16[256,1024]{1,0:T(8,128)(2,1)}, u32[]{:S(2)}) copy-start(bf16[256,1024]{1,0:T(8,128)(2,1)} %copy-done.4) | copy-start | bytes 1572868
  114.4 49.7 %collective-permute-start.18 = (bf16[512,1024]{1,0:T(8,128)(2,1)}, bf16[512,1024]{1,0:T(8,128)(2,1)S(1)}, u32[]{:S(2)}, u32[]{:S(2)}) collective-permute-start(bf16[512,1024]{1,0:T(8,128)(2,1)} %constant_dynamic-slice_fusion.1), channel_id=1, source_target_pairs={{0,8},{4,12},{8,0},{12,4},{1,9},{5,13},{9,1},{13,5},{2,10},{6,14},... | collective-permute-start | bytes 3145736 | tf_op jit(solution)/shard_map/ppermute | solution.py:88
  116.0 58.0 %collective-permute-start.17 = (bf16[512,1024]{1,0:T(8,128)(2,1)}, bf16[512,1024]{1,0:T(8,128)(2,1)}, u32[]{:S(2)}, u32[]{:S(2)}) collective-permute-start(bf16[512,1024]{1,0:T(8,128)(2,1)} %constant_dynamic-slice_fusion.1), channel_id=1, source_target_pairs={{0,4},{4,0},{8,12},{12,8},{1,5},{5,1},{9,13},{13,9},{2,6},{6,2},{1... | collective-permute-start | bytes 3145736 | tf_op jit(solution)/shard_map/ppermute | solution.py:88
  118.7 92.0 %collective-permute-start.20 = (bf16[1024,256]{1,0:T(8,128)(2,1)S(1)}, bf16[1024,256]{1,0:T(8,128)(2,1)S(1)}, u32[]{:S(2)}, u32[]{:S(2)}) collective-permute-start(bf16[1024,256]{1,0:T(8,128)(2,1)S(1)} %get-tuple-element.40), channel_id=1, source_target_pairs={{0,8},{4,12},{8,0},{12,4},{1,9},{5,13},{9,1},{13,5},{2,10},{6,14},... | collective-permute-start | bytes 1572872 | tf_op jit(solution)/shard_map/ppermute | solution.py:88
  120.3 90.8 %collective-permute-start.23 = (bf16[1024,256]{1,0:T(8,128)(2,1)S(1)}, bf16[1024,256]{1,0:T(8,128)(2,1)S(1)}, u32[]{:S(2)}, u32[]{:S(2)}) collective-permute-start(bf16[1024,256]{1,0:T(8,128)(2,1)S(1)} %get-tuple-element.40), channel_id=1, source_target_pairs={{0,4},{4,0},{8,12},{12,8},{1,5},{5,1},{9,13},{13,9},{2,6},{6,2},{1... | collective-permute-start | bytes 1572872 | tf_op jit(solution)/shard_map/ppermute | solution.py:88
  164.1 44.4 %collective-permute-start.19 = (bf16[512,1024]{1,0:T(8,128)(2,1)S(1)}, bf16[512,1024]{1,0:T(8,128)(2,1)S(1)}, u32[]{:S(2)}, u32[]{:S(2)}) collective-permute-start(bf16[512,1024]{1,0:T(8,128)(2,1)S(1)} %collective-permute-done.18), channel_id=1, source_target_pairs={{0,4},{4,0},{8,12},{12,8},{1,5},{5,1},{9,13},{13,9},{2,6},{6,2},{1... | collective-permute-start | bytes 3145736 | tf_op jit(solution)/shard_map/ppermute | solution.py:88
  176.5 33.5 %copy-start.12 = (bf16[2048,512]{1,0:T(8,128)(2,1)S(1)}, bf16[2048,512]{1,0:T(8,128)(2,1)}, u32[]{:S(2)}) copy-start(bf16[2048,512]{1,0:T(8,128)(2,1)} %param.12) | copy-start | bytes 6291460
  211.7 2.7 collective-permute-start.24
  216.2 14.0 %collective-permute-start.25 = (bf16[256,1024]{1,0:T(8,128)(2,1)S(1)}, bf16[256,1024]{1,0:T(8,128)(2,1)S(1)}, u32[]{:S(2)}, u32[]{:S(2)}) collective-permute-start(bf16[256,1024]{1,0:T(8,128)(2,1)S(1)} %pad_maximum_fusion.9), channel_id=1, source_target_pairs={{0,16},{16,0},{1,17},{17,1},{2,18},{18,2},{3,19},{19,3},{4,20},{20... | collective-permute-start | bytes 1572872 | tf_op jit(solution)/shard_map/ppermute | solution.py:88
  217.7 24.8 %collective-permute-start.22 = (bf16[1024,256]{1,0:T(8,128)(2,1)S(1)}, bf16[1024,256]{1,0:T(8,128)(2,1)S(1)}, u32[]{:S(2)}, u32[]{:S(2)}) collective-permute-start(bf16[1024,256]{1,0:T(8,128)(2,1)S(1)} %get-tuple-element.41), channel_id=1, source_target_pairs={{0,4},{4,0},{8,12},{12,8},{1,5},{5,1},{9,13},{13,9},{2,6},{6,2},{1... | collective-permute-start | bytes 1572872 | tf_op jit(solution)/shard_map/ppermute | solution.py:88
  218.5 25.6 %collective-permute-start.26 = (bf16[1024,256]{1,0:T(8,128)(2,1)S(1)}, bf16[1024,256]{1,0:T(8,128)(2,1)S(1)}, u32[]{:S(2)}, u32[]{:S(2)}) collective-permute-start(bf16[1024,256]{1,0:T(8,128)(2,1)S(1)} %get-tuple-element.41), channel_id=1, source_target_pairs={{0,8},{4,12},{8,0},{12,4},{1,9},{5,13},{9,1},{13,5},{2,10},{6,14},... | collective-permute-start | bytes 1572872 | tf_op jit(solution)/shard_map/ppermute | solution.py:88
  244.6 2.0 collective-permute-start.27
  244.7 14.3 %collective-permute-start.21 = (bf16[1024,256]{1,0:T(8,128)(2,1)S(1)}, bf16[1024,256]{1,0:T(8,128)(2,1)S(1)}, u32[]{:S(2)}, u32[]{:S(2)}) collective-permute-start(bf16[1024,256]{1,0:T(8,128)(2,1)S(1)} %collective-permute-done.20), channel_id=1, source_target_pairs={{0,4},{4,0},{8,12},{12,8},{1,5},{5,1},{9,13},{13,9},{2,6},{6,2},{1... | collective-permute-start | bytes 1572872 | tf_op jit(solution)/shard_map/ppermute | solution.py:88
  247.5 8.4 %collective-permute-start.28 = (bf16[256,512]{1,0:T(8,128)(2,1)S(1)}, bf16[256,512]{1,0:T(8,128)(2,1)S(1)}, u32[]{:S(2)}, u32[]{:S(2)}) collective-permute-start(bf16[256,512]{1,0:T(8,128)(2,1)S(1)} %pad_maximum_fusion.14), channel_id=1, source_target_pairs={{0,16},{16,0},{1,17},{17,1},{2,18},{18,2},{3,19},{19,3},{4,20},{20... | collective-permute-start | bytes 786440 | tf_op jit(solution)/shard_map/ppermute | solution.py:88
  259.5 1.6 collective-permute-start.29
  259.5 14.3 %collective-permute-start.32 = (bf16[1024,256]{1,0:T(8,128)(2,1)S(1)}, bf16[1024,256]{1,0:T(8,128)(2,1)S(1)}, u32[]{:S(2)}, u32[]{:S(2)}) collective-permute-start(bf16[1024,256]{1,0:T(8,128)(2,1)S(1)} %collective-permute-done.26), channel_id=1, source_target_pairs={{0,4},{4,0},{8,12},{12,8},{1,5},{5,1},{9,13},{13,9},{2,6},{6,2},{1... | collective-permute-start | bytes 1572872 | tf_op jit(solution)/shard_map/ppermute | solution.py:88
  261.5 5.6 %collective-permute-start.30 = (bf16[256,256]{1,0:T(8,128)(2,1)S(1)}, bf16[256,256]{1,0:T(8,128)(2,1)S(1)}, u32[]{:S(2)}, u32[]{:S(2)}) collective-permute-start(bf16[256,256]{1,0:T(8,128)(2,1)S(1)} %slice.387), channel_id=1, source_target_pairs={{0,16},{16,0},{1,17},{17,1},{2,18},{18,2},{3,19},{19,3},{4,20},{20... | collective-permute-start | bytes 393224 | tf_op jit(solution)/shard_map/ppermute | solution.py:88
  262.2 12.2 %collective-permute-start.36 = (bf16[128,1024]{1,0:T(8,128)(2,1)S(1)}, bf16[128,1024]{1,0:T(8,128)(2,1)S(1)}, u32[]{:S(2)}, u32[]{:S(2)}) collective-permute-start(bf16[128,1024]{1,0:T(8,128)(2,1)S(1)} %pad_maximum_fusion.15), channel_id=1, source_target_pairs={{0,2},{1,3},{2,0},{3,1},{4,6},{5,7},{6,4},{7,5},{8,10},{9,11},{10,... | collective-permute-start | bytes 786440 | tf_op jit(solution)/shard_map/ppermute | solution.py:88
  274.3 1.6 collective-permute-start.33
  274.6 11.9 %copy-start.7 = (bf16[128,512]{1,0:T(8,128)(2,1)S(1)}, bf16[128,512]{1,0:T(8,128)(2,1)}, u32[]{:S(2)}) copy-start(bf16[128,512]{1,0:T(8,128)(2,1)} %copy-done.6) | copy-start | bytes 393220
  274.6 11.9 %copy-start.9 = (bf16[128,512]{1,0:T(8,128)(2,1)S(1)}, bf16[128,512]{1,0:T(8,128)(2,1)}, u32[]{:S(2)}) copy-start(bf16[128,512]{1,0:T(8,128)(2,1)} %copy-done.8) | copy-start | bytes 393220
  274.6 11.9 %copy-start.11 = (bf16[128,512]{1,0:T(8,128)(2,1)S(1)}, bf16[128,512]{1,0:T(8,128)(2,1)}, u32[]{:S(2)}) copy-start(bf16[128,512]{1,0:T(8,128)(2,1)} %copy-done.10) | copy-start | bytes 393220
  274.6 11.9 %copy-start.16 = (f32[1,512]{1,0:T(1,128)S(1)}, f32[1,512]{1,0:T(1,128)}, u32[]{:S(2)}) copy-start(f32[1,512]{1,0:T(1,128)} %get-tuple-element.70) | copy-start | bytes 6148
  274.6 11.9 %copy-start.17 = (f32[1,512]{1,0:T(1,128)S(1)}, f32[1,512]{1,0:T(1,128)}, u32[]{:S(2)}) copy-start(f32[1,512]{1,0:T(1,128)} %get-tuple-element.74) | copy-start | bytes 6148
  274.7 6.0 %collective-permute-start.37 = (bf16[128,512]{1,0:T(8,128)(2,1)S(1)}, bf16[128,512]{1,0:T(8,128)(2,1)S(1)}, u32[]{:S(2)}, u32[]{:S(2)}) collective-permute-start(bf16[128,512]{1,0:T(8,128)(2,1)S(1)} %pad_maximum_fusion.17), channel_id=1, source_target_pairs={{0,2},{1,3},{2,0},{3,1},{4,6},{5,7},{6,4},{7,5},{8,10},{9,11},{10,... | collective-permute-start | bytes 393224 | tf_op jit(solution)/shard_map/ppermute | solution.py:88
  276.4 5.6 %collective-permute-start.34 = (bf16[256,256]{1,0:T(8,128)(2,1)S(1)}, bf16[256,256]{1,0:T(8,128)(2,1)S(1)}, u32[]{:S(2)}, u32[]{:S(2)}) collective-permute-start(bf16[256,256]{1,0:T(8,128)(2,1)S(1)} %slice.391), channel_id=1, source_target_pairs={{0,16},{16,0},{1,17},{17,1},{2,18},{18,2},{3,19},{19,3},{4,20},{20... | collective-permute-start | bytes 393224 | tf_op jit(solution)/shard_map/ppermute | solution.py:88
  280.9 4.5 %collective-permute-start.31 = (bf16[128,256]{1,0:T(8,128)(2,1)S(1)}, bf16[128,256]{1,0:T(8,128)(2,1)S(1)}, u32[]{:S(2)}, u32[]{:S(2)}) collective-permute-start(bf16[128,256]{1,0:T(8,128)(2,1)S(1)} %slice.389), channel_id=1, source_target_pairs={{0,2},{1,3},{2,0},{3,1},{4,6},{5,7},{6,4},{7,5},{8,10},{9,11},{10,... | collective-permute-start | bytes 196616 | tf_op jit(solution)/shard_map/ppermute | solution.py:88
  282.0 4.3 %collective-permute-start.35 = (bf16[128,256]{1,0:T(8,128)(2,1)S(1)}, bf16[128,256]{1,0:T(8,128)(2,1)S(1)}, u32[]{:S(2)}, u32[]{:S(2)}) collective-permute-start(bf16[128,256]{1,0:T(8,128)(2,1)S(1)} %slice.393), channel_id=1, source_target_pairs={{0,2},{1,3},{2,0},{3,1},{4,6},{5,7},{6,4},{7,5},{8,10},{9,11},{10,... | collective-permute-start | bytes 196616 | tf_op jit(solution)/shard_map/ppermute | solution.py:88
  (9 other events, 73.1 us)
